TPU v7x, 256 devices: a whole 4x4x8 slice. The times are simulated.
256 devices in a mesh: sp: 64 (over z, y, core), tp: 4 (over x).
Axes of the slice: x: 4, y: 4, z: 8, core: 2. Of those that a mesh axis runs over, the one named last changes fastest.
Arguments:
- cotangent: bfloat16 [8192, 2048], P('sp', 'tp'), may hold values from -16 to 16
- mixer_out: bfloat16 [8192, 2048], P('sp', 'tp'), may hold values from -6 to 6
- route_ids: int32 [8192, 2], P('sp'), may hold values from 0 to 63, all different within a row; in each aligned block of 128 rows (0 to 127, 128 to 255, ...) at most 8 rows name the same one
- route_weights: float32 [8192, 2], P('sp'), may hold values from 0.2 to 1
- conv_out: bfloat16 [8192, 2048], P('sp', 'tp'), may hold values from -6 to 6
- recur_gate: bfloat16 [8192, 2048], P('sp', 'tp'), may hold values from 0.007 to 1
- input_gate: bfloat16 [8192, 2048], P('sp', 'tp'), may hold values from 0.099609375 to 0.8984375
- gate_pre: bfloat16 [8192, 2048], P('sp', 'tp'), may hold values from -6 to 6
- states_before: bfloat16 [8192, 2048], P('sp', 'tp'), may hold values from -4 to 4
- decay_rate: float32 [2048], P('tp'), may hold values from 4e-07 to 0.008
- out_proj: bfloat16 [2048, 2048], P(None, 'tp'), may hold values from -0.125 to 0.125
- recur_map: bfloat16 [4, 512, 512], P('tp'), may hold values from -0.25 to 0.25
- input_map: bfloat16 [4, 512, 512], P('tp'), may hold values from -0.25 to 0.25
- expert_gate: bfloat16 [64, 2048, 1024], P('sp', None, 'tp'), may hold values from -0.125 to 0.125
- expert_up: bfloat16 [64, 2048, 1024], P('sp', None, 'tp'), may hold values from -0.125 to 0.125
- expert_down: bfloat16 [64, 1024, 2048], P('sp', 'tp'), may hold values from -0.1875 to 0.1875
Outputs:
- grad_expert_gate: bfloat16 [64, 2048, 1024], P('sp', None, 'tp')
- grad_expert_up: bfloat16 [64, 2048, 1024], P('sp', None, 'tp')
- grad_expert_down: bfloat16 [64, 1024, 2048], P('sp', 'tp')
- grad_out_proj: float32 [2048, 2048], P('sp', 'tp')
- grad_conv: bfloat16 [8192, 2048], P('sp', 'tp')
- grad_gate_pre: bfloat16 [8192, 2048], P('sp', 'tp')
Inputs may be any that keep to these rules, and one draw needn't show every extreme that they name: `route_ids`: the two experts of a token differ. In every aligned block of 128 tokens no expert is named by more than 8 routes, and in some block some expert by exactly 8.
All inputs are finite; a program needn't handle non-finite values.
Results may differ from a plain program's by a relative error of at most 0.0093.
Values may be sent and summed in bfloat16 or wider, within the bound.
A program may use at most 64 MiB of HBM per device.

v0:
```python
import jax
import jax.numpy as jnp
from jax import lax
from jax.sharding import Mesh
from jax.sharding import PartitionSpec as P

SP = ("sp_0", "sp_1", "sp_2")


def sent_together(arrays, axis, split_dim, concat_dim, along):
    widths = [a.shape[along] for a in arrays]
    both = jnp.concatenate(arrays, axis=along)
    whole = lax.all_to_all(both, axis, split_axis=split_dim, concat_axis=concat_dim, tiled=True)
    return tuple(jnp.split(whole, [sum(widths[:k]) for k in range(1, len(widths))], axis=along))


def laid_out(pieces, dim):
    pieces = jnp.moveaxis(pieces, 0, dim)
    shape = pieces.shape
    return pieces.reshape(*shape[:dim], shape[dim] * shape[dim + 1], *shape[dim + 2 :])


def from_everyone(shard, axis):
    devices = lax.axis_size(axis)
    return lax.all_to_all(
        jnp.broadcast_to(shard[None], (devices, *shard.shape)), axis, 0, 0, tiled=True
    )


def gathered_copies(shard, axis, dim):
    return laid_out(from_everyone(shard, axis), dim)


def side_by_side(arrays, axis, dim, along):
    ends, at = ([], 0)
    for a in arrays[:-1]:
        at += a.shape[along]
        ends.append(at)
    both = jnp.concatenate(arrays, axis=along)
    return tuple(jnp.split(gathered_copies(both, axis, dim), ends, axis=along))


def cut_along(shard, dim, devices):
    before, after = (shard.shape[:dim], shard.shape[dim + 1 :])
    return jnp.moveaxis(shard.reshape(*before, devices, -1, *after), dim, 0)


def sent_and_summed(shard, axis, dim):
    pieces = cut_along(shard, dim, lax.axis_size(axis))
    arrived = lax.all_to_all(pieces, axis, split_axis=0, concat_axis=0, tiled=True)
    return arrived.astype(jnp.float32).sum(axis=0)


def summed_rows(shard, axes, dim):
    far, near = axes
    own = sent_and_summed(cut_along(shard, dim, lax.axis_size(far)), near, dim + 1)
    return jnp.sum(
        lax.all_to_all(own.astype(jnp.bfloat16), far, 0, 0, tiled=True).astype(jnp.float32), axis=0
    )


def all_in_one(shard, axis):
    leaves = jax.tree.leaves(shard)
    order = sorted(range(len(leaves)), key=lambda k: -leaves[k].size)
    width = (1, *leaves[order[0]].shape)[-1]
    lines = [
        jnp.pad(leaves[k].reshape(-1), (0, -leaves[k].size % width)).reshape(-1, width)
        for k in order
    ]
    both, at, found = (from_everyone(jnp.concatenate(lines), axis), 0, {})
    for k, line in zip(order, lines):
        share = both[:, at : at + len(line)].reshape(len(both), -1)
        found[k] = share[:, : leaves[k].size].reshape(-1, *leaves[k].shape)
        at += len(line)
    numbers = iter(range(len(leaves)))
    return jax.tree.map(lambda _: found[next(numbers)], shard)


def joined_by_halves(pieces, combine):
    while len(jax.tree.leaves(pieces)[0]) > 1:
        pieces = jax.vmap(combine)(
            *(jax.tree.map(lambda part: part[side::2], pieces) for side in (0, 1))
        )
    return jax.tree.map(lambda part: part[0], pieces)


def carried_in(shard, axis, combine, identity):
    devices, place = (lax.axis_size(axis), lax.axis_index(axis))
    passed = jnp.arange(devices) > place

    def kept(part, zero, own):
        part = jnp.where(
            passed.reshape(-1, *(1 for _ in own.shape)), part, jnp.asarray(zero, own.dtype)
        )
        return part[::-1]

    pieces = all_in_one(shard, axis)
    return joined_by_halves(jax.tree.map(kept, pieces, identity, shard), combine)


def silu_parts(values):
    sig = jax.nn.sigmoid(values)
    return (values * sig, sig * (1.0 + values * (1.0 - sig)))


def route_slots(route_block, experts, capacity):
    flat_ids = route_block.reshape(-1)
    onehot = (flat_ids[:, None] == jnp.arange(experts, dtype=jnp.int32)[None, :]).astype(jnp.int32)
    before = jnp.cumsum(onehot, axis=0) - onehot
    slot_rank = jnp.sum(before * onehot, axis=1)
    return flat_ids * capacity + slot_rank


def link_steps(earlier, later):
    return (earlier[0] * later[0], later[0] * earlier[1] + later[1])


def join_carry(earlier, later):
    return (later[0] * earlier[0], later[1] + later[0] * earlier[1])


def contract_rows(left, right):
    return lax.dot_general(
        left, right, (((0,), (0,)), ((), ())), preferred_element_type=jnp.float32
    )


def body(
    cotangent,
    mixer_out,
    route_ids,
    route_weights,
    conv_out,
    recur_gate,
    input_gate,
    gate_pre,
    states_before,
    decay_rate,
    out_proj,
    recur_map,
    input_map,
    expert_gate,
    expert_up,
    expert_down,
):
    row_count = cotangent.shape[0]
    experts = lax.axis_size(SP)
    capacity = 4 * row_count // experts
    slot_pos = route_slots(route_ids, experts, capacity).reshape(row_count, 2)
    slot_range = jnp.arange(experts * capacity, dtype=jnp.int32)[:, None]
    hit_first = slot_range == slot_pos[None, :, 0]
    hit_second = slot_range == slot_pos[None, :, 1]
    dispatch = (hit_first | hit_second).astype(jnp.bfloat16)
    slot_weight = jnp.sum(
        jnp.where(hit_first, route_weights[None, :, 0], 0.0)
        + jnp.where(hit_second, route_weights[None, :, 1], 0.0),
        axis=1,
    )
    send_rows = jnp.dot(dispatch, mixer_out, preferred_element_type=jnp.float32).astype(
        jnp.bfloat16
    )
    send_cot = (
        jnp.dot(dispatch, cotangent, preferred_element_type=jnp.float32) * slot_weight[:, None]
    ).astype(jnp.bfloat16)
    send_rows, send_cot = (send_rows, send_cot)
    part_rows, part_cot = sent_together((send_rows, send_cot), SP, 0, 0, 1)
    got_rows, got_cot = side_by_side((part_rows, part_cot), "tp", 1, 0)
    w_gate = expert_gate[0]
    w_up = expert_up[0]
    w_down = expert_down[0]
    pre_gate = jnp.dot(got_rows, w_gate, preferred_element_type=jnp.float32)
    pre_up = jnp.dot(got_rows, w_up, preferred_element_type=jnp.float32)
    gate_act, slope = silu_parts(pre_gate)
    active = (gate_act * pre_up).astype(jnp.bfloat16)
    d_active = lax.dot_general(
        got_cot, w_down, (((1,), (1,)), ((), ())), preferred_element_type=jnp.float32
    )
    grad_down = contract_rows(active, got_cot).astype(jnp.bfloat16)
    d_gate = (d_active * pre_up * slope).astype(jnp.bfloat16)
    d_up = (d_active * gate_act).astype(jnp.bfloat16)
    grad_gate = contract_rows(got_rows, d_gate).astype(jnp.bfloat16)
    grad_up = contract_rows(got_rows, d_up).astype(jnp.bfloat16)
    partial_grad = lax.dot_general(
        d_gate, w_gate, (((1,), (1,)), ((), ())), preferred_element_type=jnp.float32
    ) + lax.dot_general(d_up, w_up, (((1,), (1,)), ((), ())), preferred_element_type=jnp.float32)
    summed = sent_and_summed(partial_grad.astype(jnp.bfloat16), "tp", 1).astype(jnp.bfloat16)
    returned = lax.all_to_all(summed, SP, split_axis=0, concat_axis=0, tiled=True)
    grad_part = (cotangent.astype(jnp.float32) + contract_rows(dispatch, returned)).astype(
        jnp.bfloat16
    )
    out_grad = gathered_copies(grad_part, "tp", 1)
    channels = conv_out.shape[1]
    rate = decay_rate[None, :]
    recur_f = recur_gate.astype(jnp.float32)
    input_f = input_gate.astype(jnp.float32)
    conv_f = conv_out.astype(jnp.float32)
    before_f = states_before.astype(jnp.float32)
    log_decay = -8.0 * recur_f * rate
    decay_now = jnp.exp(log_decay)
    position = lax.axis_index(SP) * row_count + jnp.arange(row_count, dtype=jnp.int32)
    at_start = (position == 0)[:, None]
    norm_factor = jnp.where(at_start, 1.0, jnp.sqrt(-jnp.expm1(2.0 * log_decay)))
    norm_slope = jnp.where(at_start, 0.0, -jnp.exp(2.0 * log_decay) / norm_factor)
    drive = input_f * conv_f
    state = decay_now * before_f + norm_factor * drive
    gate, gelu_back = jax.vjp(jax.nn.gelu, gate_pre.astype(jnp.float32))
    mixed = (state * gate).astype(jnp.bfloat16)
    d_mixed = jnp.dot(out_grad, out_proj, preferred_element_type=jnp.float32)
    grad_out_proj = summed_rows(
        contract_rows(out_grad, mixed).astype(jnp.bfloat16), (("sp_0", "sp_1"), "sp_2"), 0
    )
    grad_gate_pre = gelu_back(d_mixed * state)[0].astype(jnp.bfloat16)
    decay_next = jnp.concatenate([decay_now[1:], jnp.ones((1, channels), jnp.float32)], axis=0)
    carry_weight, local_grad = lax.associative_scan(
        link_steps, (decay_next, d_mixed * gate), axis=0, reverse=True
    )
    span_decay = decay_now[0] * carry_weight[0]
    span_start = decay_now[0] * local_grad[0]
    identity = (jnp.ones((channels,), jnp.float32), jnp.zeros((channels,), jnp.float32))
    _, incoming = carried_in((span_decay, span_start), SP, join_carry, identity)
    state_grad = local_grad + carry_weight * incoming[None, :]
    d_log = state_grad * (decay_now * before_f + norm_slope * drive)
    d_recur_pre = (d_log * (-8.0 * rate) * recur_f * (1.0 - recur_f)).astype(jnp.bfloat16)
    d_input_pre = (state_grad * norm_factor * conv_f * input_f * (1.0 - input_f)).astype(
        jnp.bfloat16
    )
    groups = recur_map.shape[0]
    width = recur_map.shape[1]
    through_recur = jnp.einsum(
        "tbj,bij->tbi",
        d_recur_pre.reshape(row_count, groups, width),
        recur_map,
        preferred_element_type=jnp.float32,
    )
    through_input = jnp.einsum(
        "tbj,bij->tbi",
        d_input_pre.reshape(row_count, groups, width),
        input_map,
        preferred_element_type=jnp.float32,
    )
    grad_conv = (
        state_grad * norm_factor * input_f
        + (through_recur + through_input).reshape(row_count, channels)
    ).astype(jnp.bfloat16)
    return (
        grad_gate[None],
        grad_up[None],
        grad_down[None],
        grad_out_proj,
        grad_conv,
        grad_gate_pre,
    )


def solution(mesh):
    torus = Mesh(mesh.devices.reshape(8, 4, 2, mesh.shape["tp"]), ("sp_0", "sp_1", "sp_2", "tp"))
    in_specs = (
        P(SP, "tp"),
        P(SP, "tp"),
        P(SP, None),
        P(SP, None),
        P(SP, "tp"),
        P(SP, "tp"),
        P(SP, "tp"),
        P(SP, "tp"),
        P(SP, "tp"),
        P("tp"),
        P(None, "tp"),
        P("tp", None, None),
        P("tp", None, None),
        P(SP, None, "tp"),
        P(SP, None, "tp"),
        P(SP, "tp", None),
    )
    out_specs = (
        P(SP, None, "tp"),
        P(SP, None, "tp"),
        P(SP, "tp", None),
        P(SP, "tp"),
        P(SP, "tp"),
        P(SP, "tp"),
    )
    return jax.shard_map(body, mesh=torus, in_specs=in_specs, out_specs=out_specs, check_vma=False)
```

profile of v0, /device:TPU:1, one launch (start us, length us, event | category | flops | bytes accessed | tf_op | source)
XLA Modules:
  0.0 257.9 jit_solution(15503749882287219339)
XLA Ops:
  0.6 0.9 copy.61
  4.5 1.2 convolution_convert_fusion.4
  5.9 1.2 fusion.3
  7.2 1.3 copy.65
  8.5 41.3 %all_to_all.54 = bf16[64,8,1024]{2,1,0:T(8,128)(2,1)S(1)} all-to-all(bf16[64,8,1024]{2,1,0:T(8,128)(2,1)} %bitcast.109), channel_id=1, replica_groups=mesh['sp_0'=8,'sp_1'=4,'sp_2'=2,'tp'=4] {'sp_0','sp_1','sp_2'}, dimensions={0} | all-to-all | bytes 2097152 | tf_op jit(solution)/shard_map/all_to_all | solution.py:13
  49.9 1.0 pad_maximum_fusion.1
  51.0 1.5 copy.66
  53.0 51.0 %all_to_all.55 = bf16[4,1024,512]{1,2,0:T(8,128)(2,1)S(1)} all-to-all(bf16[4,1024,512]{1,2,0:T(8,128)(2,1)S(1)} %broadcast_in_dim.98), channel_id=1, replica_groups=mesh['sp_0'=8,'sp_1'=4,'sp_2'=2,'tp'=4] {'tp'}, dimensions={0} | all-to-all | bytes 8388608 | tf_op jit(solution)/shard_map/all_to_all | solution.py:25
  104.4 0.8 copy-done.2
  107.9 0.8 multiply_convert_fusion.1
  110.5 27.1 %all_to_all.56 = bf16[4,512,512]{2,1,0:T(8,128)(2,1)} all-to-all(bf16[4,512,512]{2,1,0:T(8,128)(2,1)S(1)} %bitcast.106), channel_id=1, replica_groups=mesh['sp_0'=8,'sp_1'=4,'sp_2'=2,'tp'=4] {'tp'}, dimensions={0} | all-to-all | bytes 4194304 | tf_op jit(solution)/shard_map/all_to_all | solution.py:50
  137.5 2.9 %reduce_sum.56 = bf16[512,512]{1,0:T(8,128)(2,1)} reduce(bf16[4,512,512]{2,1,0:T(8,128)(2,1)} %all_to_all.56, bf16[]{:T(256)} %constant.23.clone.1), dimensions={0}, to_apply=%region_4.5 | reduce | flops 786432 | bytes 2621442 | tf_op jit(solution)/shard_map/reduce_sum | solution.py:51
  140.4 9.9 %all-to-all-start.3 = ((bf16[64,8,512]{2,1,0:T(8,128)(2,1)}), bf16[64,8,512]{2,1,0:T(8,128)(2,1)S(1)}, u32[]{:S(2)}, u32[]{:S(2)}) async-start(bf16[64,8,512]{2,1,0:T(8,128)(2,1)} %bitcast.17), calls=%async_computation.3 | async-start | bytes 1048576 | tf_op jit(solution)/shard_map/all_to_all | solution.py:187
  150.3 17.6 %all-to-all-done.3 = bf16[64,8,512]{2,1,0:T(8,128)(2,1)S(1)} async-done(((bf16[64,8,512]{2,1,0:T(8,128)(2,1)}), bf16[64,8,512]{2,1,0:T(8,128)(2,1)S(1)}, u32[]{:S(2)}, u32[]{:S(2)}) %all-to-all-start.3) | async-done | bytes 524320 | tf_op jit(solution)/shard_map/all_to_all | solution.py:187
  168.4 0.9 broadcast_in_dim.102
  169.3 3.7 %all-to-all-start.4 = ((bf16[4,128,512]{1,2,0:T(8,128)(2,1)}), bf16[4,128,512]{1,2,0:T(8,128)(2,1)S(1)}, u32[]{:S(2)}, u32[]{:S(2)}) async-start(bf16[4,128,512]{1,2,0:T(8,128)(2,1)} %broadcast_in_dim.102), calls=%async_computation.4 | async-start | bytes 1048576 | tf_op jit(solution)/shard_map/all_to_all | solution.py:25
  173.0 3.3 %fusion = bf16[1,2048,256]{2,1,0:T(8,128)(2,1)} fusion(bf16[512,2048]{0,1:T(8,128)(2,1)} %bitcast.101, bf16[512,256]{1,0:T(8,128)(2,1)S(1)} %get-tuple-element.9), kind=kOutput, calls=%fused_computation.5 | convolution fusion | flops 537395200 | bytes 3407872 | tf_op jit(solution)/shard_map/dot_general | solution.py:123
  176.4 5.5 %all-to-all-done.4 = bf16[4,128,512]{1,2,0:T(8,128)(2,1)S(1)} async-done(((bf16[4,128,512]{1,2,0:T(8,128)(2,1)}), bf16[4,128,512]{1,2,0:T(8,128)(2,1)S(1)}, u32[]{:S(2)}, u32[]{:S(2)}) %all-to-all-start.4) | async-done | bytes 524320 | tf_op jit(solution)/shard_map/all_to_all | solution.py:25
  181.9 2.4 convolution_convert_fusion
  184.4 1.5 fusion.37
  188.7 3.2 %copy.83 = bf16[32,2,32,512]{3,2,0,1:T(8,128)(2,1)} copy(bf16[32,2,32,512]{3,2,1,0:T(8,128)(2,1)} %bitcast.105) | data formatting | bytes 4194304 | tf_op jit(solution)/shard_map/reshape;reshape | solution.py:45
  191.9 6.1 %all-to-all-start.5 = ((bf16[2,32,32,512]{3,2,1,0:T(8,128)(2,1)}), bf16[2,32,32,512]{3,2,1,0:T(8,128)(2,1)}, u32[]{:S(2)}, u32[]{:S(2)}) async-start(bf16[2,32,32,512]{3,2,1,0:T(8,128)(2,1)} %bitcast.104), calls=%async_computation.5 | async-start | bytes 4194304 | tf_op jit(solution)/shard_map/all_to_all | solution.py:50
  201.4 5.5 %all-to-all-start.7 = ((f32[64,2,512]{2,1,0:T(2,128)}), f32[64,2,512]{2,1,0:T(2,128)}, u32[]{:S(2)}, u32[]{:S(2)}) async-start(f32[64,2,512]{2,1,0:T(2,128)} %broadcast_in_dim.106), calls=%async_computation.7 | async-start | bytes 524288 | tf_op jit(solution)/shard_map/all_to_all | solution.py:25
  206.9 3.4 %fusion.1 = bf16[1,2048,256]{2,1,0:T(8,128)(2,1)} fusion(bf16[512,2048]{0,1:T(8,128)(2,1)} %bitcast.102, bf16[512,256]{1,0:T(8,128)(2,1)S(1)} %copy-done.15), kind=kOutput, calls=%fused_computation.6 | convolution fusion | flops 537395200 | bytes 3407872 | tf_op jit(solution)/shard_map/dot_general | solution.py:123
  210.3 1.7 fusion.2
  212.2 1.4 rev.4
  213.6 1.4 rev.5
  214.9 3.4 %reduce_sum.57 = bf16[32,32,512]{2,1,0:T(8,128)(2,1)} reduce(bf16[2,32,32,512]{3,2,1,0:T(8,128)(2,1)} %all-to-all-done.5, bf16[]{:T(256)} %constant.23.clone.1), dimensions={0}, to_apply=%region_5.6 | reduce | flops 524288 | bytes 3145730 | tf_op jit(solution)/shard_map/reduce_sum | solution.py:51
  218.3 1.6 all-to-all-done.7
  219.9 7.9 %all-to-all-start.6 = ((bf16[32,32,512]{2,1,0:T(8,128)(2,1)}), bf16[32,32,512]{2,1,0:T(8,128)(2,1)S(1)}, u32[]{:S(2)}, u32[]{:S(2)}) async-start(bf16[32,32,512]{2,1,0:T(8,128)(2,1)} %reduce_sum.57), calls=%async_computation.6 | async-start | bytes 2097152 | tf_op jit(solution)/shard_map/all_to_all | solution.py:58
  227.8 1.3 fusion.103
  229.2 1.3 slice.427
  230.6 1.3 slice.424
  231.8 1.2 slice.429
  233.1 1.6 fusion.105
  234.7 1.5 slice.433
  236.1 1.4 slice.436
  238.8 1.5 fusion.107
  240.3 1.4 slice.437
  241.6 1.4 slice.440
  243.0 1.4 slice.435
  244.4 1.4 slice.438
  245.7 1.4 fusion.109
  247.1 1.3 slice.441
  248.4 1.3 slice.444
  253.0 0.8 multiply_add_fusion.13
  253.8 2.0 fusion.17
  255.9 1.2 fusion.6
  (227 shorter events, 20.2 us)
Async XLA Ops:
  0.6 183.7 %copy-start = (bf16[2048,512]{1,0:T(8,128)(2,1)S(1)}, bf16[2048,512]{1,0:T(8,128)(2,1)}, u32[]{:S(2)}) copy-start(bf16[2048,512]{1,0:T(8,128)(2,1)} %param.26) | copy-start | bytes 6291460
  104.0 1.2 copy-start.2
  104.4 2.9 %copy-start.1 = (bf16[512,4,512]{0,2,1:T(8,128)(2,1)}, bf16[512,4,512]{0,2,1:T(8,128)(2,1)S(1)}, u32[]{:S(2)}) copy-start(bf16[512,4,512]{0,2,1:T(8,128)(2,1)S(1)} %get-tuple-element.7) | copy-start | bytes 6291460
  104.4 2.9 %copy-start.4 = (bf16[512,4,512]{0,2,1:T(8,128)(2,1)}, bf16[512,4,512]{0,2,1:T(8,128)(2,1)S(1)}, u32[]{:S(2)}) copy-start(bf16[512,4,512]{0,2,1:T(8,128)(2,1)S(1)} %get-tuple-element.6) | copy-start | bytes 6291460
  104.4 2.1 copy-start.3
  106.5 2.2 copy-start.6
  106.5 1.4 copy-start.31
  107.3 1.5 copy-start.8
  108.8 0.8 copy-start.14
  137.5 12.8 %copy-start.28 = (f32[512]{0:T(512)S(1)}, f32[512]{0:T(512)}, u32[]{:S(2)}) copy-start(f32[512]{0:T(512)} %param.25) | copy-start | bytes 6148
  137.5 30.5 %copy-start.10 = (bf16[128,512]{1,0:T(8,128)(2,1)S(1)}, bf16[128,512]{1,0:T(8,128)(2,1)}, u32[]{:S(2)}) copy-start(bf16[128,512]{1,0:T(8,128)(2,1)} %param.16) | copy-start | bytes 393220
  140.4 27.6 %all-to-all-start.3 = ((bf16[64,8,512]{2,1,0:T(8,128)(2,1)}), bf16[64,8,512]{2,1,0:T(8,128)(2,1)S(1)}, u32[]{:S(2)}, u32[]{:S(2)}) async-start(bf16[64,8,512]{2,1,0:T(8,128)(2,1)} %bitcast.17), calls=%async_computation.3 | async-start | bytes 1048576 | tf_op jit(solution)/shard_map/all_to_all | solution.py:187
  150.3 34.0 %copy-start.26 = (f32[512]{0:T(512)}, f32[512]{0:T(512)S(1)}, u32[]{:S(2)}) copy-start(f32[512]{0:T(512)S(1)} %broadcast_multiply_fusion) | copy-start | bytes 6148
  169.3 12.6 %all-to-all-start.4 = ((bf16[4,128,512]{1,2,0:T(8,128)(2,1)}), bf16[4,128,512]{1,2,0:T(8,128)(2,1)S(1)}, u32[]{:S(2)}, u32[]{:S(2)}) async-start(bf16[4,128,512]{1,2,0:T(8,128)(2,1)} %broadcast_in_dim.102), calls=%async_computation.4 | async-start | bytes 1048576 | tf_op jit(solution)/shard_map/all_to_all | solution.py:25
  173.0 11.4 %copy-start.29 = (pred[128]{0:T(512)(128)(4,1)}, pred[128]{0:T(512)(128)(4,1)S(1)}, u32[]{:S(2)}) copy-start(pred[128]{0:T(512)(128)(4,1)S(1)} %add_compare_fusion) | copy-start | bytes 388
  173.0 8.9 %copy-start.16 = (bf16[128,512]{1,0:T(8,128)(2,1)S(1)}, bf16[128,512]{1,0:T(8,128)(2,1)}, u32[]{:S(2)}) copy-start(bf16[128,512]{1,0:T(8,128)(2,1)} %param.23) | copy-start | bytes 393220
  173.0 8.9 %copy-start.17 = (bf16[128,512]{1,0:T(8,128)(2,1)S(1)}, bf16[128,512]{1,0:T(8,128)(2,1)}, u32[]{:S(2)}) copy-start(bf16[128,512]{1,0:T(8,128)(2,1)} %param.24) | copy-start | bytes 393220
  173.0 8.9 %copy-start.18 = (bf16[128,512]{1,0:T(8,128)(2,1)S(1)}, bf16[128,512]{1,0:T(8,128)(2,1)}, u32[]{:S(2)}) copy-start(bf16[128,512]{1,0:T(8,128)(2,1)} %param.20) | copy-start | bytes 393220
  173.0 8.9 %copy-start.20 = (bf16[128,512]{1,0:T(8,128)(2,1)S(1)}, bf16[128,512]{1,0:T(8,128)(2,1)}, u32[]{:S(2)}) copy-start(bf16[128,512]{1,0:T(8,128)(2,1)} %param.22) | copy-start | bytes 393220
  173.0 8.9 %copy-start.23 = (bf16[128,512]{1,0:T(8,128)(2,1)S(1)}, bf16[128,512]{1,0:T(8,128)(2,1)}, u32[]{:S(2)}) copy-start(bf16[128,512]{1,0:T(8,128)(2,1)} %param.21) | copy-start | bytes 393220
  176.4 8.0 %copy-start.21 = (bf16[128,512]{1,0:T(8,128)(2,1)S(1)}, bf16[128,512]{1,0:T(8,128)(2,1)}, u32[]{:S(2)}) copy-start(bf16[128,512]{1,0:T(8,128)(2,1)} %param.22) | copy-start | bytes 393220
  176.4 8.0 %copy-start.24 = (bf16[128,512]{1,0:T(8,128)(2,1)S(1)}, bf16[128,512]{1,0:T(8,128)(2,1)}, u32[]{:S(2)}) copy-start(bf16[128,512]{1,0:T(8,128)(2,1)} %param.21) | copy-start | bytes 393220
  185.8 0.7 copy-start.11
  191.9 8.7 %all-to-all-start.5 = ((bf16[2,32,32,512]{3,2,1,0:T(8,128)(2,1)}), bf16[2,32,32,512]{3,2,1,0:T(8,128)(2,1)}, u32[]{:S(2)}, u32[]{:S(2)}) async-start(bf16[2,32,32,512]{3,2,1,0:T(8,128)(2,1)} %bitcast.104), calls=%async_computation.5 | async-start | bytes 4194304 | tf_op jit(solution)/shard_map/all_to_all | solution.py:50
  199.1 7.8 %copy-start.15 = (bf16[512,256]{1,0:T(8,128)(2,1)S(1)}, bf16[512,256]{1,0:T(8,128)(2,1)}, u32[]{:S(2)}) copy-start(bf16[512,256]{1,0:T(8,128)(2,1)} %copy-done.14) | copy-start | bytes 786436
  201.4 18.5 %all-to-all-start.7 = ((f32[64,2,512]{2,1,0:T(2,128)}), f32[64,2,512]{2,1,0:T(2,128)}, u32[]{:S(2)}, u32[]{:S(2)}) async-start(f32[64,2,512]{2,1,0:T(2,128)} %broadcast_in_dim.106), calls=%async_computation.7 | async-start | bytes 524288 | tf_op jit(solution)/shard_map/all_to_all | solution.py:25
  206.9 3.5 %copy-start.5 = (bf16[512,4,512]{0,2,1:T(8,128)(2,1)S(1)}, bf16[512,4,512]{0,2,1:T(8,128)(2,1)}, u32[]{:S(2)}) copy-start(bf16[512,4,512]{0,2,1:T(8,128)(2,1)} %copy-done.4) | copy-start | bytes 6291460
  206.9 3.4 %copy-start.7 = (f32[512,256]{1,0:T(8,128)S(1)}, f32[512,256]{1,0:T(8,128)}, u32[]{:S(2)}) copy-start(f32[512,256]{1,0:T(8,128)} %copy-done.6) | copy-start | bytes 1572868
  206.9 3.4 %copy-start.9 = (f32[512,256]{1,0:T(8,128)S(1)}, f32[512,256]{1,0:T(8,128)}, u32[]{:S(2)}) copy-start(f32[512,256]{1,0:T(8,128)} %copy-done.8) | copy-start | bytes 1572868
  219.9 37.2 %all-to-all-start.6 = ((bf16[32,32,512]{2,1,0:T(8,128)(2,1)}), bf16[32,32,512]{2,1,0:T(8,128)(2,1)S(1)}, u32[]{:S(2)}, u32[]{:S(2)}) async-start(bf16[32,32,512]{2,1,0:T(8,128)(2,1)} %reduce_sum.57), calls=%async_computation.6 | async-start | bytes 2097152 | tf_op jit(solution)/shard_map/all_to_all | solution.py:58
  233.1 22.7 %copy-start.12 = (f32[128,512]{1,0:T(8,128)S(1)}, f32[128,512]{1,0:T(8,128)}, u32[]{:S(2)}) copy-start(f32[128,512]{1,0:T(8,128)} %rev.4) | copy-start | bytes 786436
  238.8 17.0 %copy-start.19 = (bf16[128,512]{1,0:T(8,128)(2,1)S(1)}, bf16[128,512]{1,0:T(8,128)(2,1)}, u32[]{:S(2)}) copy-start(bf16[128,512]{1,0:T(8,128)(2,1)} %param.20) | copy-start | bytes 393220
  253.0 2.8 %copy-start.13 = (f32[128,512]{1,0:T(8,128)S(1)}, f32[128,512]{1,0:T(8,128)}, u32[]{:S(2)}) copy-start(f32[128,512]{1,0:T(8,128)} %rev.5) | copy-start | bytes 786436
  253.0 2.8 %copy-start.22 = (bf16[128,512]{1,0:T(8,128)(2,1)S(1)}, bf16[128,512]{1,0:T(8,128)(2,1)}, u32[]{:S(2)}) copy-start(bf16[128,512]{1,0:T(8,128)(2,1)} %param.22) | copy-start | bytes 393220
  253.0 2.8 %copy-start.25 = (bf16[128,512]{1,0:T(8,128)(2,1)S(1)}, bf16[128,512]{1,0:T(8,128)(2,1)}, u32[]{:S(2)}) copy-start(bf16[128,512]{1,0:T(8,128)(2,1)} %param.21) | copy-start | bytes 393220
  253.0 2.8 %copy-start.27 = (f32[512]{0:T(512)S(1)}, f32[512]{0:T(512)}, u32[]{:S(2)}) copy-start(f32[512]{0:T(512)} %copy-done.26) | copy-start | bytes 6148
  253.0 2.8 %copy-start.30 = (pred[128]{0:T(512)(128)(4,1)S(1)}, pred[128]{0:T(512)(128)(4,1)}, u32[]{:S(2)}) copy-start(pred[128]{0:T(512)(128)(4,1)} %copy-done.29) | copy-start | bytes 388
  253.0 2.8 %copy-start.32 = (bf16[1,512,512]{2,1,0:T(8,128)(2,1)S(1)}, bf16[1,512,512]{2,1,0:T(8,128)(2,1)}, u32[]{:S(2)}) copy-start(bf16[1,512,512]{2,1,0:T(8,128)(2,1)} %param.28) | copy-start | bytes 1572868
where the time goes:
time: 260 us; the launch traced here: 258 us
  blocking collectives  119 us (46%)
  local copies, waits for them, and re-layouts  39.2 us (15%)
  starting transfers between devices  33 us (13%)
  waiting for transfers between devices  25.2 us (10%)
  matrix products  22.1 us (8%)
  other arithmetic  17.2 us (7%)
    all_to_all x1, blocking collectives, from_everyone(): lax.all_to_all(jnp.broadcast_to(shard[None], (devices, *shard.shape)), ax...  51 us
    all_to_all x1, blocking collectives, sent_together(): lax.all_to_all(both, axis, split_axis=split_dim, concat_axis=concat_dim,...  41.3 us
    all_to_all x1, blocking collectives, sent_and_summed(): lax.all_to_all(pieces, axis, split_axis=0, concat_axis=0, tiled=True)  27.1 us
    slice x24, local copies, waits for them, and re-layouts, joined_by_halves(): part[side::2]  18.6 us
    all_to_all x1, waiting for transfers between devices, body(): lax.all_to_all(summed, SP, split_axis=0, concat_axis=0, tiled=True)  17.6 us
    dot_general x5, matrix products, contract_rows(): lax.dot_general(left, right, (((0,), (0,)), ((), ())), preferred_element_...  11.2 us
    all_to_all x1, starting transfers between devices, body(): lax.all_to_all(summed, SP, split_axis=0, concat_axis=0, tiled=True)  9.87 us
    all_to_all x2, starting transfers between devices, from_everyone(): lax.all_to_all(jnp.broadcast_to(shard[None], (devices, *shard.shape)), ax...  9.15 us
  transfers between devices with their start and end apart: 5, of which 4 were waited for; matrix products, arithmetic and copies ran while one was open for 18% of the time, Pallas kernels for 0%

commit v1 on v0

--- a/solution.py
+++ b/solution.py
@@ -1,10 +1,271 @@
+import functools
+
 import jax
 import jax.numpy as jnp
 from jax import lax
+from jax.experimental import pallas as pl
+from jax.experimental.pallas import tpu as pltpu
 from jax.sharding import Mesh
 from jax.sharding import PartitionSpec as P
 
 SP = ("sp_0", "sp_1", "sp_2")
+
+
+MESH_ID = pl.DeviceIdType.MESH
+AXES = (*SP, "tp")
+
+
+def near_first(count):
+    return sorted(range(count), key=lambda k: (min(k, count - k), k))
+
+
+def slot_hits(ids, experts, capacity):
+    tokens = ids.shape[1]
+    slots = experts * capacity
+    first, second = ids[0:1, :], ids[1:2, :]
+    expert = lax.broadcasted_iota(jnp.int32, (experts, tokens), 0)
+    named = jnp.where((expert == first) | (expert == second), 1.0, 0.0).astype(jnp.bfloat16)
+    at = lax.broadcasted_iota(jnp.int32, (tokens, tokens), 0)
+    later = lax.broadcasted_iota(jnp.int32, (tokens, tokens), 1)
+    earlier = jnp.where(at < later, 1.0, 0.0).astype(jnp.bfloat16)
+    before = jnp.dot(named, earlier, preferred_element_type=jnp.float32)
+    of_slot = lax.broadcasted_iota(jnp.int32, (slots, experts), 0)
+    of_expert = lax.broadcasted_iota(jnp.int32, (slots, experts), 1)
+    spread = jnp.where(of_slot // capacity == of_expert, 1.0, 0.0).astype(jnp.bfloat16)
+    rank = jnp.dot(spread, before.astype(jnp.bfloat16), preferred_element_type=jnp.float32)
+    slot = lax.broadcasted_iota(jnp.int32, (slots, tokens), 0)
+    free = rank == (slot % capacity).astype(jnp.float32)
+    return free & (slot // capacity == first), free & (slot // capacity == second)
+
+
+def dispatch_kernel(
+    sizes, ids_ref, weights_ref, mixer_ref, cot_ref, rows_ref, cots_ref, hits_ref,
+    send_rows, send_cots, a_send, a_recv, own_send, own_recv, pass_send, pass_recv, met,
+):
+    nz, ny, nc, nx = sizes
+    plane = ny * nc
+    z, y, c, x = (lax.axis_index(a) for a in AXES)
+    width = cot_ref.shape[1]
+    right, left = lax.rem(x + 1, nx), lax.rem(x + nx - 1, nx)
+    across = lax.rem(x + 2, nx)
+    me = (z * ny + y) * nc + c
+
+    def partner(j, sign):
+        dz, dy, dc = j // plane, (j // nc) % ny, j % nc
+        return (
+            lax.rem(z + sign * dz + nz, nz),
+            lax.rem(y + sign * dy + ny, ny),
+            lax.rem(c + sign * dc + nc, nc),
+        )
+
+    barrier = pltpu.get_barrier_semaphore()
+
+    def greet(sem, first, stop, step):
+        def one(k, carry):
+            pl.semaphore_signal(
+                sem, inc=1, device_id=(*partner(k * step, 1), x), device_id_type=MESH_ID
+            )
+            return carry
+
+        lax.fori_loop(first, stop, one, 0)
+
+    greet(barrier, 1, nz, plane)
+    greet(barrier, 1, plane, 1)
+    for side in (left, right):
+        pl.semaphore_signal(barrier, inc=1, device_id=(z, y, c, side), device_id_type=MESH_ID)
+
+    experts = nz * plane
+    first, second = slot_hits(ids_ref[...], experts, rows_ref.shape[1])
+    hits = jnp.where(first | second, 1.0, 0.0).astype(jnp.bfloat16)
+    hits_ref[...] = hits
+    weights = weights_ref[...]
+    weight = jnp.sum(
+        jnp.where(first, weights[0:1, :], 0.0) + jnp.where(second, weights[1:2, :], 0.0),
+        axis=1,
+        keepdims=True,
+    )
+    shape = send_rows.shape
+    rows = jnp.dot(hits, mixer_ref[...], preferred_element_type=jnp.float32)
+    send_rows[...] = rows.reshape(shape).astype(jnp.bfloat16)
+    cots = jnp.dot(hits, cot_ref[...], preferred_element_type=jnp.float32) * weight
+    send_cots[...] = cots.reshape(shape).astype(jnp.bfloat16)
+
+    pl.semaphore_wait(barrier, nz - 1 + plane - 1 + 2)
+    greet(met, 1, plane, 1)
+    pl.semaphore_wait(met, plane - 1)
+
+    def columns(part):
+        return pl.ds(pl.multiple_of(part * width, width), width)
+
+    pairs = ((send_rows, rows_ref), (send_cots, cots_ref))
+
+    def local(k):
+        source, target = pairs[k]
+        return pltpu.make_async_copy(
+            source.at[me], target.at[me, :, columns(x)], a_recv.at[k, 0]
+        )
+
+    def sent(k, j):
+        dz, dy, dc = partner(j, 1)
+        source, target = pairs[k]
+        return pltpu.make_async_remote_copy(
+            src_ref=source.at[(dz * ny + dy) * nc + dc],
+            dst_ref=target.at[me, :, columns(x)],
+            send_sem=a_send.at[k, j],
+            recv_sem=a_recv.at[k, j],
+            device_id=(dz, dy, dc, x),
+            device_id_type=MESH_ID,
+        )
+
+    def arriving(k, j):
+        sz, sy, sc = partner(j, -1)
+        source, target = pairs[k]
+        return pltpu.make_async_remote_copy(
+            src_ref=source.at[me],
+            dst_ref=target.at[(sz * ny + sy) * nc + sc, :, columns(x)],
+            send_sem=a_send.at[k, j],
+            recv_sem=a_recv.at[k, j],
+            device_id=(sz, sy, sc, x),
+            device_id_type=MESH_ID,
+        )
+
+    for k in (0, 1):
+        local(k).start()
+    order = near_first(nz)
+    for dz in order:
+
+        def send(j, carry):
+            for k in (0, 1):
+                sent(k, j).start()
+            return carry
+
+        lax.fori_loop(max(dz * plane, 1), (dz + 1) * plane, send, 0)
+
+    def block(ref, dz, half, part):
+        start = lax.rem(z - dz + nz, nz) * plane
+        count = plane
+        if half is not None:
+            count = plane // 2
+            start = start + half * count
+        return ref.at[pl.ds(start, count), :, columns(part)]
+
+    def own(k, dz, way):
+        ref = pairs[k][1]
+        here = block(ref, dz, None, x)
+        return pltpu.make_async_remote_copy(
+            src_ref=here,
+            dst_ref=here,
+            send_sem=own_send.at[way, k, dz],
+            recv_sem=own_recv.at[way, k, dz],
+            device_id=(z, y, c, (right, left)[way]),
+            device_id_type=MESH_ID,
+        )
+
+    def own_here(k, dz, way):
+        ref = pairs[k][1]
+        here = block(ref, dz, None, (left, right)[way])
+        return pltpu.make_async_remote_copy(
+            src_ref=here,
+            dst_ref=here,
+            send_sem=own_send.at[way, k, dz],
+            recv_sem=own_recv.at[way, k, dz],
+            device_id=(z, y, c, (left, right)[way]),
+            device_id_type=MESH_ID,
+        )
+
+    def passed(k, dz, way):
+        ref = pairs[k][1]
+        here = block(ref, dz, way, (left, right)[way])
+        return pltpu.make_async_remote_copy(
+            src_ref=here,
+            dst_ref=here,
+            send_sem=pass_send.at[way, k, dz],
+            recv_sem=pass_recv.at[way, k, dz],
+            device_id=(z, y, c, (right, left)[way]),
+            device_id_type=MESH_ID,
+        )
+
+    def passed_here(k, dz, way):
+        ref = pairs[k][1]
+        here = block(ref, dz, way, across)
+        return pltpu.make_async_remote_copy(
+            src_ref=here,
+            dst_ref=here,
+            send_sem=pass_send.at[way, k, dz],
+            recv_sem=pass_recv.at[way, k, dz],
+            device_id=(z, y, c, (left, right)[way]),
+            device_id_type=MESH_ID,
+        )
+
+    def hand_on(dz):
+        for k in (0, 1):
+            for way in (0, 1):
+                own_here(k, dz, way).wait_recv()
+                passed(k, dz, way).start()
+
+    for at, dz in enumerate(order):
+        if dz == 0:
+            for k in (0, 1):
+                local(k).wait()
+
+        def arrive(j, carry):
+            for k in (0, 1):
+                arriving(k, j).wait_recv()
+            return carry
+
+        lax.fori_loop(max(dz * plane, 1), (dz + 1) * plane, arrive, 0)
+        for k in (0, 1):
+            for way in (0, 1):
+                own(k, dz, way).start()
+        if at:
+            hand_on(order[at - 1])
+    hand_on(order[-1])
+    for dz in order:
+        for k in (0, 1):
+            for way in (0, 1):
+                passed_here(k, dz, way).wait_recv()
+
+    def drain(j, carry):
+        for k in (0, 1):
+            sent(k, j).wait_send()
+        return carry
+
+    lax.fori_loop(1, nz * plane, drain, 0)
+    for dz in order:
+        for k in (0, 1):
+            for way in (0, 1):
+                own(k, dz, way).wait_send()
+                passed(k, dz, way).wait_send()
+
+
+def dispatched(ids, weights, mixer_out, cotangent):
+    sizes = tuple(lax.axis_size(a) for a in AXES)
+    nz, ny, nc, nx = sizes
+    experts = nz * ny * nc
+    tokens, width = cotangent.shape
+    capacity = 4 * tokens // experts
+    full = jax.ShapeDtypeStruct((experts, capacity, nx * width), jnp.bfloat16)
+    vmem = pl.BlockSpec(memory_space=pltpu.VMEM)
+    dma = pltpu.SemaphoreType.DMA
+    return pl.pallas_call(
+        functools.partial(dispatch_kernel, sizes),
+        out_shape=(full, full, jax.ShapeDtypeStruct((experts * capacity, tokens), jnp.bfloat16)),
+        in_specs=[vmem] * 4,
+        out_specs=(vmem,) * 3,
+        scratch_shapes=[
+            pltpu.VMEM((experts, capacity, width), jnp.bfloat16),
+            pltpu.VMEM((experts, capacity, width), jnp.bfloat16),
+            dma((2, experts)),
+            dma((2, experts)),
+            dma((2, 2, nz)),
+            dma((2, 2, nz)),
+            dma((2, 2, nz)),
+            dma((2, 2, nz)),
+            pltpu.SemaphoreType.REGULAR,
+        ],
+        compiler_params=pltpu.CompilerParams(collective_id=0, has_side_effects=True),
+        name="dispatch",
+    )(ids.T, weights.T, mixer_out, cotangent)
 
 
 def sent_together(arrays, axis, split_dim, concat_dim, along):
@@ -144,27 +405,9 @@
     expert_down,
 ):
     row_count = cotangent.shape[0]
-    experts = lax.axis_size(SP)
-    capacity = 4 * row_count // experts
-    slot_pos = route_slots(route_ids, experts, capacity).reshape(row_count, 2)
-    slot_range = jnp.arange(experts * capacity, dtype=jnp.int32)[:, None]
-    hit_first = slot_range == slot_pos[None, :, 0]
-    hit_second = slot_range == slot_pos[None, :, 1]
-    dispatch = (hit_first | hit_second).astype(jnp.bfloat16)
-    slot_weight = jnp.sum(
-        jnp.where(hit_first, route_weights[None, :, 0], 0.0)
-        + jnp.where(hit_second, route_weights[None, :, 1], 0.0),
-        axis=1,
-    )
-    send_rows = jnp.dot(dispatch, mixer_out, preferred_element_type=jnp.float32).astype(
-        jnp.bfloat16
-    )
-    send_cot = (
-        jnp.dot(dispatch, cotangent, preferred_element_type=jnp.float32) * slot_weight[:, None]
-    ).astype(jnp.bfloat16)
-    send_rows, send_cot = (send_rows, send_cot)
-    part_rows, part_cot = sent_together((send_rows, send_cot), SP, 0, 0, 1)
-    got_rows, got_cot = side_by_side((part_rows, part_cot), "tp", 1, 0)
+    got_rows, got_cot, dispatch = dispatched(route_ids, route_weights, mixer_out, cotangent)
+    got_rows = got_rows.reshape(-1, got_rows.shape[2])
+    got_cot = got_cot.reshape(got_rows.shape)
     w_gate = expert_gate[0]
     w_up = expert_up[0]
     w_down = expert_down[0]

time: 260 us -> 219 us (0.84)
  blocking collectives: 119 us -> 28 us
  Pallas kernels: 0 us -> 62.5 us
  local copies, waits for them, and re-layouts: 39.2 us -> 32.9 us
  other arithmetic: 17.2 us -> 14.5 us
    all_to_all x2 -> x0, blocking collectives: 92.3 us -> none  [the longest x1 51 us: from_everyone(): lax.all_to_all(jnp.broadcast_to(shard[None], (devices, *shard.shape)), ax...]
    pallas_call x0 -> x1, Pallas kernels: none -> 62.5 us  [dispatched(): pl.pallas_call(functools.partial(dispatch_kernel, sizes), out_shape=(full...]
    concatenate x2 -> x0, local copies, waits for them, and re-layouts: 2.8 us -> none  [the longest x1 1.48 us: side_by_side(): both = jnp.concatenate(arrays, axis=along)]
  transfers between devices with their start and end apart: 5 -> 5, of which waited for: 4 -> 4; matrix products, arithmetic and copies ran while one was open for 18% -> 21% of each run, Pallas kernels for 0% -> 0%
where the time goes in v1:
time: 219 us; the launch traced here: 218 us
  Pallas kernels  62.5 us (29%)
  local copies, waits for them, and re-layouts  32.9 us (15%)
  starting transfers between devices  31.6 us (14%)
  blocking collectives  28 us (13%)
  waiting for transfers between devices  25.1 us (11%)
  matrix products  21.7 us (10%)
  other arithmetic  14.5 us (7%)
    pallas_call x1, Pallas kernels, dispatched(): pl.pallas_call(functools.partial(dispatch_kernel, sizes), out_shape=(full...  62.5 us
    all_to_all x1, blocking collectives, sent_and_summed(): lax.all_to_all(pieces, axis, split_axis=0, concat_axis=0, tiled=True)  28 us
    slice x24, local copies, waits for them, and re-layouts, joined_by_halves(): part[side::2]  18.7 us
    all_to_all x1, waiting for transfers between devices, body(): lax.all_to_all(summed, SP, split_axis=0, concat_axis=0, tiled=True)  17.6 us
    dot_general x5, matrix products, contract_rows(): lax.dot_general(left, right, (((0,), (0,)), ((), ())), preferred_element_...  11.3 us
    all_to_all x2, starting transfers between devices, from_everyone(): lax.all_to_all(jnp.broadcast_to(shard[None], (devices, *shard.shape)), ax...  9.15 us
    all_to_all x1, starting transfers between devices, body(): lax.all_to_all(summed, SP, split_axis=0, concat_axis=0, tiled=True)  8.41 us
    all_to_all x1, starting transfers between devices, summed_rows(): lax.all_to_all(own.astype(jnp.bfloat16), far, 0, 0, tiled=True)  7.93 us
  transfers between devices with their start and end apart: 5, of which 4 were waited for; matrix products, arithmetic and copies ran while one was open for 21% of the time, Pallas kernels for 0%

profile of v1, /device:TPU:1, one launch (start us, length us, event | category | flops | bytes accessed | tf_op | source)
XLA Modules:
  0.0 218.0 jit_solution(18147704591248116225)
XLA Ops:
  0.7 62.5 %dispatch.1 = (bf16[64,8,2048]{2,1,0:T(8,128)(2,1)}, bf16[64,8,2048]{2,1,0:T(8,128)(2,1)}, bf16[512,128]{1,0:T(8,128)(2,1)}) custom-call(s32[2,128]{1,0:T(2,128)} %bitcast.86, f32[2,128]{1,0:T(2,128)} %bitcast.87, bf16[128,512]{1,0:T(8,128)(2,1)} %mixer_ref.1, bf16[128,512]{1,0:T(8,128)(2,1)} %cot_ref.1), custom_call_target="tpu_custom_call" | custom-call | tf_op jit(solution)/shard_map/dispatch/pallas_call | solution.py:250
  63.2 2.7 %fusion.8 = f32[512,256]{1,0:T(8,128)S(1)} fusion(bf16[64,8,2048]{2,1,0:T(8,128)(2,1)} %get-tuple-element.9, bf16[1,2048,256]{2,1,0:T(8,128)(2,1)} %param.29), kind=kOutput, calls=%fused_computation.14 | convolution fusion | flops 536870912 | bytes 3670016 | tf_op jit(solution)/shard_map/dot_general | solution.py:414
  66.7 1.2 copy-done.1
  68.2 0.8 multiply_convert_fusion.1
  69.4 0.7 fusion.15
  70.2 0.8 add_convert_fusion
  71.1 28.0 %all_to_all.37 = bf16[4,512,512]{2,1,0:T(8,128)(2,1)} all-to-all(bf16[4,512,512]{2,1,0:T(8,128)(2,1)S(1)} %bitcast.80), channel_id=1, replica_groups=mesh['sp_0'=8,'sp_1'=4,'sp_2'=2,'tp'=4] {'tp'}, dimensions={0} | all-to-all | bytes 4194304 | tf_op jit(solution)/shard_map/all_to_all | solution.py:311
  99.1 2.9 %reduce_sum.33 = bf16[512,512]{1,0:T(8,128)(2,1)} reduce(bf16[4,512,512]{2,1,0:T(8,128)(2,1)} %all_to_all.37, bf16[]{:T(256)} %constant.20.clone.1), dimensions={0}, to_apply=%region_0.0 | reduce | flops 786432 | bytes 2621442 | tf_op jit(solution)/shard_map/reduce_sum | solution.py:312
  102.0 8.4 %all-to-all-start.1 = ((bf16[64,8,512]{2,1,0:T(8,128)(2,1)}), bf16[64,8,512]{2,1,0:T(8,128)(2,1)S(1)}, u32[]{:S(2)}, u32[]{:S(2)}) async-start(bf16[64,8,512]{2,1,0:T(8,128)(2,1)} %bitcast.11), calls=%async_computation.1 | async-start | bytes 1048576 | tf_op jit(solution)/shard_map/all_to_all | solution.py:430
  110.4 17.6 %all-to-all-done.1 = bf16[64,8,512]{2,1,0:T(8,128)(2,1)S(1)} async-done(((bf16[64,8,512]{2,1,0:T(8,128)(2,1)}), bf16[64,8,512]{2,1,0:T(8,128)(2,1)S(1)}, u32[]{:S(2)}, u32[]{:S(2)}) %all-to-all-start.1) | async-done | bytes 524320 | tf_op jit(solution)/shard_map/all_to_all | solution.py:430
  128.5 0.9 broadcast_in_dim.65
  129.3 3.7 %all-to-all-start.2 = ((bf16[4,128,512]{1,2,0:T(8,128)(2,1)}), bf16[4,128,512]{1,2,0:T(8,128)(2,1)S(1)}, u32[]{:S(2)}, u32[]{:S(2)}) async-start(bf16[4,128,512]{1,2,0:T(8,128)(2,1)} %broadcast_in_dim.65), calls=%async_computation.2 | async-start | bytes 1048576 | tf_op jit(solution)/shard_map/all_to_all | solution.py:286
  133.1 3.4 %fusion = bf16[1,2048,256]{2,1,0:T(8,128)(2,1)} fusion(bf16[512,256]{1,0:T(8,128)(2,1)S(1)} %get-tuple-element.13, bf16[64,8,2048]{2,1,0:T(8,128)(2,1)} %get-tuple-element.9), kind=kOutput, calls=%fused_computation.5 | convolution fusion | flops 537395200 | bytes 3407872 | tf_op jit(solution)/shard_map/dot_general | solution.py:384
  136.5 5.5 %all-to-all-done.2 = bf16[4,128,512]{1,2,0:T(8,128)(2,1)S(1)} async-done(((bf16[4,128,512]{1,2,0:T(8,128)(2,1)}), bf16[4,128,512]{1,2,0:T(8,128)(2,1)S(1)}, u32[]{:S(2)}, u32[]{:S(2)}) %all-to-all-start.2) | async-done | bytes 524320 | tf_op jit(solution)/shard_map/all_to_all | solution.py:286
  142.0 2.4 %convolution_convert_fusion = bf16[2048,512]{1,0:T(8,128)(2,1)} fusion(bf16[128,2048]{0,1:T(8,128)(2,1)S(1)} %bitcast.82, bf16[128,512]{1,0:T(8,128)(2,1)S(1)} %copy-done.15, bf16[128,512]{1,0:T(8,128)(2,1)S(1)} %copy-done.17, bf16[128,512]{1,0:T(8,128)(2,1)S(1)} %copy-done.19, bf16[128,512]{1,0:T(8,128)(2,1)S(1)} %copy-done.22, ...), kind=kOutput, calls=%fused_computation.1 | convolution fusion | flops 270991360 | bytes 3278976 | tf_op jit(solution)/shard_map/dot_general | solution.py:384
  144.4 1.5 fusion.42
  148.7 3.2 %copy.41 = bf16[32,2,32,512]{3,2,0,1:T(8,128)(2,1)} copy(bf16[32,2,32,512]{3,2,1,0:T(8,128)(2,1)} %bitcast.79) | data formatting | bytes 4194304 | tf_op jit(solution)/shard_map/reshape;reshape | solution.py:306
  151.9 6.1 %all-to-all-start.3 = ((bf16[2,32,32,512]{3,2,1,0:T(8,128)(2,1)}), bf16[2,32,32,512]{3,2,1,0:T(8,128)(2,1)}, u32[]{:S(2)}, u32[]{:S(2)}) async-start(bf16[2,32,32,512]{3,2,1,0:T(8,128)(2,1)} %bitcast.78), calls=%async_computation.3 | async-start | bytes 4194304 | tf_op jit(solution)/shard_map/all_to_all | solution.py:311
  159.5 0.7 add_multiply_fusion.11
  160.7 0.8 broadcast_in_dim.69
  161.4 5.5 %all-to-all-start.5 = ((f32[64,2,512]{2,1,0:T(2,128)}), f32[64,2,512]{2,1,0:T(2,128)}, u32[]{:S(2)}, u32[]{:S(2)}) async-start(f32[64,2,512]{2,1,0:T(2,128)} %broadcast_in_dim.69), calls=%async_computation.5 | async-start | bytes 524288 | tf_op jit(solution)/shard_map/all_to_all | solution.py:286
  167.0 3.5 %fusion.1 = bf16[1,2048,256]{2,1,0:T(8,128)(2,1)} fusion(bf16[512,256]{1,0:T(8,128)(2,1)S(1)} %copy-done.14, bf16[64,8,2048]{2,1,0:T(8,128)(2,1)} %get-tuple-element.9), kind=kOutput, calls=%fused_computation.6 | convolution fusion | flops 537395200 | bytes 3407872 | tf_op jit(solution)/shard_map/dot_general | solution.py:384
  170.4 1.8 fusion.2
  172.3 1.4 rev.4
  173.7 1.3 rev.5
  175.0 3.4 %reduce_sum.34 = bf16[32,32,512]{2,1,0:T(8,128)(2,1)} reduce(bf16[2,32,32,512]{3,2,1,0:T(8,128)(2,1)} %all-to-all-done.3, bf16[]{:T(256)} %constant.20.clone.1), dimensions={0}, to_apply=%region_1.2 | reduce | flops 524288 | bytes 3145730 | tf_op jit(solution)/shard_map/reduce_sum | solution.py:312
  178.4 1.5 all-to-all-done.5
  179.9 7.9 %all-to-all-start.4 = ((bf16[32,32,512]{2,1,0:T(8,128)(2,1)}), bf16[32,32,512]{2,1,0:T(8,128)(2,1)S(1)}, u32[]{:S(2)}, u32[]{:S(2)}) async-start(bf16[32,32,512]{2,1,0:T(8,128)(2,1)} %reduce_sum.34), calls=%async_computation.4 | async-start | bytes 2097152 | tf_op jit(solution)/shard_map/all_to_all | solution.py:319
  187.8 1.3 fusion.92
  189.3 1.3 slice.401
  190.7 1.3 slice.398
  191.9 1.2 slice.403
  193.2 1.6 fusion.94
  194.7 1.5 slice.407
  196.2 1.5 slice.410
  198.9 1.5 fusion.96
  200.4 1.4 slice.411
  201.7 1.4 slice.414
  203.1 1.4 slice.409
  204.5 1.4 slice.412
  205.8 1.4 fusion.98
  207.2 1.3 slice.415
  208.5 1.3 slice.418
  211.1 0.8 fusion.100
  213.1 0.8 multiply_add_fusion.13
  213.9 2.0 fusion.22
  216.0 1.2 fusion.14
  217.2 0.8 convert_reduce_fusion
  (204 shorter events, 10.3 us)
Async XLA Ops:
  0.6 143.8 %copy-start = (bf16[2048,512]{1,0:T(8,128)(2,1)S(1)}, bf16[2048,512]{1,0:T(8,128)(2,1)}, u32[]{:S(2)}) copy-start(bf16[2048,512]{1,0:T(8,128)(2,1)} %param.26) | copy-start | bytes 6291460
  0.6 65.3 %copy-start.4 = (bf16[1,2048,256]{2,1,0:T(8,128)(2,1)S(1)}, bf16[1,2048,256]{2,1,0:T(8,128)(2,1)}, u32[]{:S(2)}) copy-start(bf16[1,2048,256]{2,1,0:T(8,128)(2,1)} %param.30) | copy-start | bytes 3145732
  63.2 2.7 %copy-start.31 = (bf16[64,8,2048]{2,1,0:T(8,128)(2,1)S(1)}, bf16[64,8,2048]{2,1,0:T(8,128)(2,1)}, u32[]{:S(2)}) copy-start(bf16[64,8,2048]{2,1,0:T(8,128)(2,1)} %get-tuple-element.9) | copy-start | bytes 6291460
  65.9 3.1 %copy-start.6 = (f32[512,256]{1,0:T(8,128)}, f32[512,256]{1,0:T(8,128)S(1)}, u32[]{:S(2)}) copy-start(f32[512,256]{1,0:T(8,128)S(1)} %fusion.8) | copy-start | bytes 1572868
  65.9 1.9 copy-start.1
  66.0 2.2 %copy-start.32 = (bf16[1,256,2048]{2,1,0:T(8,128)(2,1)S(1)}, bf16[1,256,2048]{2,1,0:T(8,128)(2,1)}, u32[]{:S(2)}) copy-start(bf16[1,256,2048]{2,1,0:T(8,128)(2,1)} %param.31) | copy-start | bytes 3145732
  66.7 2.3 %copy-start.8 = (f32[512,256]{1,0:T(8,128)}, f32[512,256]{1,0:T(8,128)S(1)}, u32[]{:S(2)}) copy-start(f32[512,256]{1,0:T(8,128)S(1)} %fusion.10) | copy-start | bytes 1572868
  68.2 1.2 copy-start.3
  69.0 1.1 copy-start.13
  99.1 11.3 %copy-start.28 = (f32[512]{0:T(512)S(1)}, f32[512]{0:T(512)}, u32[]{:S(2)}) copy-start(f32[512]{0:T(512)} %param.25) | copy-start | bytes 6148
  99.1 29.0 %copy-start.5 = (bf16[128,512]{1,0:T(8,128)(2,1)S(1)}, bf16[128,512]{1,0:T(8,128)(2,1)}, u32[]{:S(2)}) copy-start(bf16[128,512]{1,0:T(8,128)(2,1)} %cot_ref.1) | copy-start | bytes 393220
  99.1 29.0 %copy-start.25 = (bf16[512,128]{1,0:T(8,128)(2,1)S(1)}, bf16[512,128]{1,0:T(8,128)(2,1)}, u32[]{:S(2)}) copy-start(bf16[512,128]{1,0:T(8,128)(2,1)} %get-tuple-element.11) | copy-start | bytes 393220
  102.0 26.1 %all-to-all-start.1 = ((bf16[64,8,512]{2,1,0:T(8,128)(2,1)}), bf16[64,8,512]{2,1,0:T(8,128)(2,1)S(1)}, u32[]{:S(2)}, u32[]{:S(2)}) async-start(bf16[64,8,512]{2,1,0:T(8,128)(2,1)} %bitcast.11), calls=%async_computation.1 | async-start | bytes 1048576 | tf_op jit(solution)/shard_map/all_to_all | solution.py:430
  110.4 34.0 %copy-start.26 = (f32[512]{0:T(512)}, f32[512]{0:T(512)S(1)}, u32[]{:S(2)}) copy-start(f32[512]{0:T(512)S(1)} %broadcast_multiply_fusion) | copy-start | bytes 6148
  129.3 12.6 %all-to-all-start.2 = ((bf16[4,128,512]{1,2,0:T(8,128)(2,1)}), bf16[4,128,512]{1,2,0:T(8,128)(2,1)S(1)}, u32[]{:S(2)}, u32[]{:S(2)}) async-start(bf16[4,128,512]{1,2,0:T(8,128)(2,1)} %broadcast_in_dim.65), calls=%async_computation.2 | async-start | bytes 1048576 | tf_op jit(solution)/shard_map/all_to_all | solution.py:286
  133.0 11.4 %copy-start.29 = (pred[128]{0:T(512)(128)(4,1)}, pred[128]{0:T(512)(128)(4,1)S(1)}, u32[]{:S(2)}) copy-start(pred[128]{0:T(512)(128)(4,1)S(1)} %add_compare_fusion) | copy-start | bytes 388
  133.0 8.9 %copy-start.15 = (bf16[128,512]{1,0:T(8,128)(2,1)S(1)}, bf16[128,512]{1,0:T(8,128)(2,1)}, u32[]{:S(2)}) copy-start(bf16[128,512]{1,0:T(8,128)(2,1)} %param.23) | copy-start | bytes 393220
  133.1 8.9 %copy-start.16 = (bf16[128,512]{1,0:T(8,128)(2,1)S(1)}, bf16[128,512]{1,0:T(8,128)(2,1)}, u32[]{:S(2)}) copy-start(bf16[128,512]{1,0:T(8,128)(2,1)} %param.24) | copy-start | bytes 393220
  133.1 8.9 %copy-start.17 = (bf16[128,512]{1,0:T(8,128)(2,1)S(1)}, bf16[128,512]{1,0:T(8,128)(2,1)}, u32[]{:S(2)}) copy-start(bf16[128,512]{1,0:T(8,128)(2,1)} %param.20) | copy-start | bytes 393220
  133.1 8.9 %copy-start.19 = (bf16[128,512]{1,0:T(8,128)(2,1)S(1)}, bf16[128,512]{1,0:T(8,128)(2,1)}, u32[]{:S(2)}) copy-start(bf16[128,512]{1,0:T(8,128)(2,1)} %param.22) | copy-start | bytes 393220
  133.1 8.9 %copy-start.22 = (bf16[128,512]{1,0:T(8,128)(2,1)S(1)}, bf16[128,512]{1,0:T(8,128)(2,1)}, u32[]{:S(2)}) copy-start(bf16[128,512]{1,0:T(8,128)(2,1)} %param.21) | copy-start | bytes 393220
  136.5 7.9 %copy-start.20 = (bf16[128,512]{1,0:T(8,128)(2,1)S(1)}, bf16[128,512]{1,0:T(8,128)(2,1)}, u32[]{:S(2)}) copy-start(bf16[128,512]{1,0:T(8,128)(2,1)} %param.22) | copy-start | bytes 393220
  136.5 7.9 %copy-start.23 = (bf16[128,512]{1,0:T(8,128)(2,1)S(1)}, bf16[128,512]{1,0:T(8,128)(2,1)}, u32[]{:S(2)}) copy-start(bf16[128,512]{1,0:T(8,128)(2,1)} %param.21) | copy-start | bytes 393220
  145.9 0.7 copy-start.10
  151.9 8.7 %all-to-all-start.3 = ((bf16[2,32,32,512]{3,2,1,0:T(8,128)(2,1)}), bf16[2,32,32,512]{3,2,1,0:T(8,128)(2,1)}, u32[]{:S(2)}, u32[]{:S(2)}) async-start(bf16[2,32,32,512]{3,2,1,0:T(8,128)(2,1)} %bitcast.78), calls=%async_computation.3 | async-start | bytes 4194304 | tf_op jit(solution)/shard_map/all_to_all | solution.py:311
  159.1 7.8 %copy-start.14 = (bf16[512,256]{1,0:T(8,128)(2,1)S(1)}, bf16[512,256]{1,0:T(8,128)(2,1)}, u32[]{:S(2)}) copy-start(bf16[512,256]{1,0:T(8,128)(2,1)} %copy-done.13) | copy-start | bytes 786436
  161.4 18.5 %all-to-all-start.5 = ((f32[64,2,512]{2,1,0:T(2,128)}), f32[64,2,512]{2,1,0:T(2,128)}, u32[]{:S(2)}, u32[]{:S(2)}) async-start(f32[64,2,512]{2,1,0:T(2,128)} %broadcast_in_dim.69), calls=%async_computation.5 | async-start | bytes 524288 | tf_op jit(solution)/shard_map/all_to_all | solution.py:286
  166.9 3.5 %copy-start.2 = (bf16[64,8,2048]{2,1,0:T(8,128)(2,1)S(1)}, bf16[64,8,2048]{2,1,0:T(8,128)(2,1)}, u32[]{:S(2)}) copy-start(bf16[64,8,2048]{2,1,0:T(8,128)(2,1)} %get-tuple-element.10) | copy-start | bytes 6291460
  166.9 3.5 %copy-start.7 = (f32[512,256]{1,0:T(8,128)S(1)}, f32[512,256]{1,0:T(8,128)}, u32[]{:S(2)}) copy-start(f32[512,256]{1,0:T(8,128)} %copy-done.6) | copy-start | bytes 1572868
  166.9 3.5 %copy-start.9 = (f32[512,256]{1,0:T(8,128)S(1)}, f32[512,256]{1,0:T(8,128)}, u32[]{:S(2)}) copy-start(f32[512,256]{1,0:T(8,128)} %copy-done.8) | copy-start | bytes 1572868
  179.9 37.3 %all-to-all-start.4 = ((bf16[32,32,512]{2,1,0:T(8,128)(2,1)}), bf16[32,32,512]{2,1,0:T(8,128)(2,1)S(1)}, u32[]{:S(2)}, u32[]{:S(2)}) async-start(bf16[32,32,512]{2,1,0:T(8,128)(2,1)} %reduce_sum.34), calls=%async_computation.4 | async-start | bytes 2097152 | tf_op jit(solution)/shard_map/all_to_all | solution.py:319
  193.1 22.8 %copy-start.11 = (f32[128,512]{1,0:T(8,128)S(1)}, f32[128,512]{1,0:T(8,128)}, u32[]{:S(2)}) copy-start(f32[128,512]{1,0:T(8,128)} %rev.4) | copy-start | bytes 786436
  198.9 17.0 %copy-start.18 = (bf16[128,512]{1,0:T(8,128)(2,1)S(1)}, bf16[128,512]{1,0:T(8,128)(2,1)}, u32[]{:S(2)}) copy-start(bf16[128,512]{1,0:T(8,128)(2,1)} %param.20) | copy-start | bytes 393220
  213.1 2.8 %copy-start.12 = (f32[128,512]{1,0:T(8,128)S(1)}, f32[128,512]{1,0:T(8,128)}, u32[]{:S(2)}) copy-start(f32[128,512]{1,0:T(8,128)} %rev.5) | copy-start | bytes 786436
  213.1 2.8 %copy-start.21 = (bf16[128,512]{1,0:T(8,128)(2,1)S(1)}, bf16[128,512]{1,0:T(8,128)(2,1)}, u32[]{:S(2)}) copy-start(bf16[128,512]{1,0:T(8,128)(2,1)} %param.22) | copy-start | bytes 393220
  213.1 2.8 %copy-start.24 = (bf16[128,512]{1,0:T(8,128)(2,1)S(1)}, bf16[128,512]{1,0:T(8,128)(2,1)}, u32[]{:S(2)}) copy-start(bf16[128,512]{1,0:T(8,128)(2,1)} %param.21) | copy-start | bytes 393220
  213.1 2.8 %copy-start.27 = (f32[512]{0:T(512)S(1)}, f32[512]{0:T(512)}, u32[]{:S(2)}) copy-start(f32[512]{0:T(512)} %copy-done.26) | copy-start | bytes 6148
  213.1 2.8 %copy-start.30 = (pred[128]{0:T(512)(128)(4,1)S(1)}, pred[128]{0:T(512)(128)(4,1)}, u32[]{:S(2)}) copy-start(pred[128]{0:T(512)(128)(4,1)} %copy-done.29) | copy-start | bytes 388
  213.1 2.8 %copy-start.33 = (bf16[1,512,512]{2,1,0:T(8,128)(2,1)S(1)}, bf16[1,512,512]{2,1,0:T(8,128)(2,1)}, u32[]{:S(2)}) copy-start(bf16[1,512,512]{2,1,0:T(8,128)(2,1)} %param.28) | copy-start | bytes 1572868

commit v2 on v0

v2 whole, which is shorter than its diff:
```python
import functools

import jax
import jax.numpy as jnp
from jax import lax
from jax.experimental import pallas as pl
from jax.experimental.pallas import tpu as pltpu
from jax.sharding import Mesh
from jax.sharding import PartitionSpec as P

SP = ("sp_0", "sp_1", "sp_2")
AXES = (*SP, "tp")
MESH_ID = pl.DeviceIdType.MESH
BF16 = jnp.bfloat16
F32 = jnp.float32
PIECES = 2


def near_first(count):
    return sorted(range(count), key=lambda k: (min(k, count - k), k))


def slot_hits(ids, experts, capacity):
    tokens = ids.shape[1]
    slots = experts * capacity
    first, second = ids[0:1, :], ids[1:2, :]
    expert = lax.broadcasted_iota(jnp.int32, (experts, tokens), 0)
    named = jnp.where((expert == first) | (expert == second), 1.0, 0.0).astype(jnp.bfloat16)
    at = lax.broadcasted_iota(jnp.int32, (tokens, tokens), 0)
    later = lax.broadcasted_iota(jnp.int32, (tokens, tokens), 1)
    earlier = jnp.where(at < later, 1.0, 0.0).astype(jnp.bfloat16)
    before = jnp.dot(named, earlier, preferred_element_type=jnp.float32)
    of_slot = lax.broadcasted_iota(jnp.int32, (slots, experts), 0)
    of_expert = lax.broadcasted_iota(jnp.int32, (slots, experts), 1)
    spread = jnp.where(of_slot // capacity == of_expert, 1.0, 0.0).astype(jnp.bfloat16)
    rank = jnp.dot(spread, before.astype(jnp.bfloat16), preferred_element_type=jnp.float32)
    slot = lax.broadcasted_iota(jnp.int32, (slots, tokens), 0)
    free = rank == (slot % capacity).astype(jnp.float32)
    return free & (slot // capacity == first), free & (slot // capacity == second)


def dot(left, right, at_left=1, at_right=0):
    return lax.dot_general(
        left, right, (((at_left,), (at_right,)), ((), ())), preferred_element_type=F32
    )


def layer_kernel(sizes, *refs):
    names = IN_NAMES + OUT_NAMES + SCRATCH_NAMES
    r = dict(zip(names, refs, strict=True))
    nz, ny, nc, nx = sizes
    plane = ny * nc
    experts = nz * plane
    z, y, c, x = (lax.axis_index(a) for a in AXES)
    tokens, width = r["cot"].shape
    capacity = r["rows"].shape[1]
    me = (z * ny + y) * nc + c
    mine = y * nc + c
    right, left = lax.rem(x + 1, nx), lax.rem(x + nx - 1, nx)
    across = lax.rem(x + 2, nx)
    up, down = lax.rem(y + 1, ny), lax.rem(y + ny - 1, ny)
    over = lax.rem(y + 2, ny)
    twin = nc - 1 - c
    group = plane * capacity
    order = near_first(nz)
    waits = []

    def columns(part):
        return pl.ds(pl.multiple_of(part * width, width), width)

    def partner(j, sign):
        dz, dy, dc = j // plane, (j // nc) % ny, j % nc
        return (
            lax.rem(z + sign * dz + nz, nz),
            lax.rem(y + sign * dy + ny, ny),
            lax.rem(c + sign * dc + nc, nc),
        )

    def remote(source, target, send, recv, device):
        return pltpu.make_async_remote_copy(
            src_ref=source,
            dst_ref=target,
            send_sem=send,
            recv_sem=recv,
            device_id=device,
            device_id_type=MESH_ID,
        )

    loads = {
        name: pltpu.make_async_copy(r[name], r[name + "_in"], r["load_sem"].at[k])
        for k, name in enumerate(LOADED)
    }
    for name in LOADED:
        loads[name].start()

    barrier = pltpu.get_barrier_semaphore()

    def greet(sem, first, stop, step):
        def one(k, carry):
            pl.semaphore_signal(
                sem, inc=1, device_id=(*partner(k * step, 1), x), device_id_type=MESH_ID
            )
            return carry

        lax.fori_loop(first, stop, one, 0)

    greet(barrier, 1, nz, plane)
    greet(barrier, 1, plane, 1)
    for side in (left, right):
        pl.semaphore_signal(barrier, inc=1, device_id=(z, y, c, side), device_id_type=MESH_ID)

    first, second = slot_hits(r["ids"][...], experts, capacity)
    hits = jnp.where(first | second, 1.0, 0.0).astype(BF16)
    r["hits"][...] = hits
    weights = r["weights"][...]
    weight = jnp.sum(
        jnp.where(first, weights[0:1, :], 0.0) + jnp.where(second, weights[1:2, :], 0.0),
        axis=1,
        keepdims=True,
    )
    shape = r["send_rows"].shape
    r["send_rows"][...] = dot(hits, r["mixer"][...]).reshape(shape).astype(BF16)
    r["send_cots"][...] = (dot(hits, r["cot"][...]) * weight).reshape(shape).astype(BF16)

    pl.semaphore_wait(barrier, nz - 1 + plane - 1 + 2)
    greet(r["met"], 1, plane, 1)
    pl.semaphore_wait(r["met"], plane - 1)

    pairs = ((r["send_rows"], r["rows"]), (r["send_cots"], r["cots"]))

    def local(k):
        source, target = pairs[k]
        return pltpu.make_async_copy(
            source.at[me], target.at[me, :, columns(x)], r["a_recv"].at[k, 0]
        )

    def sent(k, j):
        dz, dy, dc = partner(j, 1)
        source, target = pairs[k]
        return remote(
            source.at[(dz * ny + dy) * nc + dc],
            target.at[me, :, columns(x)],
            r["a_send"].at[k, j],
            r["a_recv"].at[k, j],
            (dz, dy, dc, x),
        )

    def arriving(k, j):
        sz, sy, sc = partner(j, -1)
        source, target = pairs[k]
        return remote(
            source.at[me],
            target.at[(sz * ny + sy) * nc + sc, :, columns(x)],
            r["a_send"].at[k, j],
            r["a_recv"].at[k, j],
            (sz, sy, sc, x),
        )

    for k in (0, 1):
        local(k).start()
    for dz in order:

        def send(j, carry):
            for k in (0, 1):
                sent(k, j).start()
            return carry

        lax.fori_loop(max(dz * plane, 1), (dz + 1) * plane, send, 0)

    for name in RECURRENCE:
        loads[name].wait()
    recur = r["recur_gate_in"][...].astype(F32)
    rate = r["decay_rate_in"][...]
    log_decay = -8.0 * recur * rate
    decay = jnp.exp(log_decay)
    norm = r["norm_in"][...]
    position = lax.broadcasted_iota(jnp.int32, (tokens, width), 0)
    at_start = (position + me * tokens) == 0
    slope = jnp.where(at_start, 0.0, -jnp.exp(2.0 * log_decay) / norm)
    conv = r["conv_in"][...].astype(F32)
    entry = r["input_gate_in"][...].astype(F32)
    drive = entry * conv
    before = r["states_in"][...].astype(F32)
    state = decay * before + norm * drive
    r["by_recur"][...] = (
        (decay * before + slope * drive) * (-8.0 * rate) * recur * (1.0 - recur)
    )
    r["by_input"][...] = norm * conv * entry * (1.0 - entry)
    r["by_conv"][...] = norm * entry
    pre = r["gate_pre_in"][...].astype(F32)
    root = 0.7978845608028654
    bent = jnp.tanh(root * (pre + 0.044715 * (pre * pre * pre)))
    cdf = 0.5 * (1.0 + bent)
    gate = pre * cdf
    gelu_slope = cdf + 0.5 * pre * (1.0 - bent * bent) * root * (1.0 + 3.0 * 0.044715 * (pre * pre))
    r["gate"][...] = gate
    r["mixed"][...] = (state * gate).astype(BF16)
    r["by_gate"][...] = state * gelu_slope
    r["first_decay"][...] = decay[0:8, :]
    following = pltpu.roll(decay, tokens - 1, 0)
    last = position == tokens - 1
    reach = jnp.where(last, 0.0, following)
    carry_weight = jnp.where(last, 1.0, following)
    step = 1
    level = 0
    while step < tokens:
        r["reach"][level] = reach
        moved = pltpu.roll(reach, tokens - step, 0)
        reach = reach * moved
        moved = pltpu.roll(carry_weight, tokens - step, 0)
        carry_weight = carry_weight * jnp.where(position < tokens - step, moved, 1.0)
        step *= 2
        level += 1
    r["carry_weight"][...] = carry_weight
    for name in LOADED:
        if name not in RECURRENCE:
            loads[name].wait()

    def start_of(dz):
        return lax.rem(z - dz + nz, nz) * plane

    def ring_block(ref, dz, half, part):
        start, count = start_of(dz), plane
        if half is not None:
            count = plane // 2
            start = start + half * count
        return ref.at[pl.ds(start, count), :, columns(part)]

    sides = (left, right)
    others = (right, left)

    def own(k, dz, way, arrives):
        here = ring_block(pairs[k][1], dz, None, sides[way] if arrives else x)
        return remote(
            here, here, r["own_send"].at[way, k, dz], r["own_recv"].at[way, k, dz],
            (z, y, c, sides[way] if arrives else others[way]),
        )

    def passed(k, dz, way, arrives):
        here = ring_block(pairs[k][1], dz, way, across if arrives else sides[way])
        return remote(
            here, here, r["pass_send"].at[way, k, dz], r["pass_recv"].at[way, k, dz],
            (z, y, c, sides[way] if arrives else others[way]),
        )

    both_ways = [(k, way) for k in (0, 1) for way in (0, 1)]

    def hand_on(dz):
        for k, way in both_ways:
            own(k, dz, way, True).wait_recv()
            passed(k, dz, way, False).start()

    def settle(dz):
        for k, way in both_ways:
            passed(k, dz, way, True).wait_recv()

    def as_rows(ref, starts, cols):
        return jnp.concatenate(
            [ref[pl.ds(s, plane), :, cols].reshape(group, -1) for s in starts], axis=0
        )

    def keep(ref, starts, cols, value):
        for k, s in enumerate(starts):
            part = value[k * group : (k + 1) * group]
            ref[pl.ds(s, plane), :, cols] = part.reshape(plane, capacity, -1).astype(BF16)

    def expert_rows(dzs):
        starts = [start_of(dz) for dz in dzs]
        for name in ("acc_gate", "acc_up", "acc_down"):
            r[name][...] = jnp.zeros_like(r[name])

        def gather(t, carry):
            cols = columns(t)
            row_part = as_rows(r["rows"], starts, cols)
            r["acc_gate"][...] += dot(row_part, r["w_gate_in"][cols, :])
            r["acc_up"][...] += dot(row_part, r["w_up_in"][cols, :])
            cot_part = as_rows(r["cots"], starts, cols)
            r["acc_down"][...] += dot(cot_part, r["w_down_in"][:, cols], 1, 1)
            return carry

        lax.fori_loop(0, nx, gather, 0)
        pre_gate, pre_up, d_active = r["acc_gate"][...], r["acc_up"][...], r["acc_down"][...]
        sig = jax.nn.sigmoid(pre_gate)
        silu = pre_gate * sig
        silu_slope = sig * (1.0 + pre_gate * (1.0 - sig))
        d_gate = d_active * pre_up * silu_slope
        d_up = d_active * silu
        whole = slice(None)
        keep(r["active"], starts, whole, silu * pre_up)
        keep(r["d_gate"], starts, whole, d_gate)
        keep(r["d_up"], starts, whole, d_up)
        d_gate, d_up = d_gate.astype(BF16), d_up.astype(BF16)

        def spread(t, carry):
            cols = columns(t)
            value = dot(d_gate, r["w_gate_in"][cols, :], 1, 1)
            value += dot(d_up, r["w_up_in"][cols, :], 1, 1)
            keep(r["partial"], starts, cols, value)
            return carry

        lax.fori_loop(0, nx, spread, 0)

    def half_sum(dz, way, arrives):
        return remote(
            ring_block(r["partial"], dz, way, across),
            r["half_in"].at[way, dz],
            r["half_send"].at[way, dz],
            r["half_recv"].at[way, dz],
            (z, y, c, sides[way] if arrives else others[way]),
        )

    def unit_sum(dz, way, arrives):
        return remote(
            r["unit_out"].at[way, dz],
            r["unit_in"].at[way, dz],
            r["unit_send"].at[way, dz],
            r["unit_recv"].at[way, dz],
            (z, y, c, sides[way] if arrives else others[way]),
        )

    def sum_one(dz):
        for way in (0, 1):
            half_sum(dz, way, False).start()

    def sum_two(dz):
        start = start_of(dz)
        for way in (0, 1):
            half_sum(dz, way, True).wait_recv()
            value = r["partial"][pl.ds(start, plane), :, columns(others[way])].astype(F32)
            more = r["half_in"][way, dz].astype(F32)
            half = plane // 2
            parts = [value[:half], value[half:]]
            parts[way] = parts[way] + more
            r["unit_out"][way, dz] = jnp.concatenate(parts, axis=0).astype(BF16)
            unit_sum(dz, way, False).start()

    def returned(j):
        dz, dy, dc = partner(j, -1)
        return remote(
            r["back_out"].at[(dz * ny + dy) * nc + dc],
            r["back_in"].at[me],
            r["back_send"].at[j],
            r["back_recv"].at[j],
            (dz, dy, dc, x),
        )

    def returning(j):
        sz, sy, sc = partner(j, 1)
        return remote(
            r["back_out"].at[me],
            r["back_in"].at[(sz * ny + sy) * nc + sc],
            r["back_send"].at[j],
            r["back_recv"].at[j],
            (sz, sy, sc, x),
        )

    def back_local():
        return pltpu.make_async_copy(
            r["back_out"].at[me], r["back_in"].at[me], r["back_recv"].at[0]
        )

    def sum_three(dz):
        start = start_of(dz)
        value = r["partial"][pl.ds(start, plane), :, columns(x)].astype(F32)
        for way in (0, 1):
            unit_sum(dz, way, True).wait_recv()
            value = value + r["unit_in"][way, dz].astype(F32)
        r["back_out"][pl.ds(start, plane)] = value.astype(BF16)

        def give(j, carry):
            returned(j).start()
            return carry

        lax.fori_loop(max(dz * plane, 1), (dz + 1) * plane, give, 0)
        if dz == 0:
            back_local().start()

    chunks = [order[k : k + 2] for k in range(0, nz, 2)]

    def sums(stage, k):
        if 0 <= k < len(chunks):
            for dz in chunks[k]:
                stage(dz)

    for at, dz in enumerate(order):
        if dz == 0:
            for k in (0, 1):
                local(k).wait()

        def arrive(j, carry):
            for k in (0, 1):
                arriving(k, j).wait_recv()
            return carry

        lax.fori_loop(max(dz * plane, 1), (dz + 1) * plane, arrive, 0)
        for k, way in both_ways:
            own(k, dz, way, False).start()
        if at:
            hand_on(order[at - 1])
        if at >= 2:
            settle(order[at - 2])
        if at >= 3 and at % 2:
            k = (at - 3) // 2
            sums(sum_two, k - 1)
            sums(sum_three, k - 2)
            expert_rows(chunks[k])
            sums(sum_one, k)
    hand_on(order[-1])
    k = len(chunks) - 1
    sums(sum_two, k - 1)
    sums(sum_three, k - 2)
    settle(order[-2])
    settle(order[-1])
    expert_rows(chunks[k])
    sums(sum_one, k)
    sums(sum_three, k - 1)

    def rows_of(name, cols):
        return r[name][:, :, cols].reshape(experts * capacity, -1)

    whole = slice(None)

    def grad_in(name):
        def part(t, carry):
            cols = columns(t)
            value = dot(rows_of("rows", cols), rows_of("d_" + name, whole), 0, 0)
            r["g_" + name][cols, :] = value.astype(BF16)
            return carry

        lax.fori_loop(0, nx, part, 0)

    def grad_down():
        def part(t, carry):
            cols = columns(t)
            value = dot(rows_of("active", whole), rows_of("cots", cols), 0, 0)
            r["g_down"][:, cols] = value.astype(BF16)
            return carry

        lax.fori_loop(0, nx, part, 0)

    stores = {
        name: pltpu.make_async_copy(r["g_" + name], r["grad_" + name], r["store_sem"].at[k])
        for k, name in enumerate(("gate", "up", "down"))
    }
    sums(sum_two, k)
    grad_in("gate")
    stores["gate"].start()
    sums(sum_three, k)
    grad_in("up")
    stores["up"].start()

    back_local().wait()

    def come(j, carry):
        returning(j).wait_recv()
        return carry

    lax.fori_loop(1, experts, come, 0)
    routed = dot(r["hits"][...], r["back_in"][...].reshape(experts * capacity, width), 0, 0)
    r["out_grad"][:, columns(x)] = (r["cot"][...].astype(F32) + routed).astype(BF16)

    half_rows = tokens // 2

    def grad_own(way, arrives):
        here = r["out_grad"].at[:, columns(sides[way] if arrives else x)]
        return remote(
            here, here, r["og_send"].at[way], r["og_recv"].at[way],
            (z, y, c, sides[way] if arrives else others[way]),
        )

    def grad_passed(way, arrives):
        here = r["out_grad"].at[
            pl.ds(way * half_rows, half_rows), columns(across if arrives else sides[way])
        ]
        return remote(
            here, here, r["og_send"].at[2 + way], r["og_recv"].at[2 + way],
            (z, y, c, sides[way] if arrives else others[way]),
        )

    for way in (0, 1):
        grad_own(way, False).start()
    grad_down()
    stores["down"].start()
    for way in (0, 1):
        grad_own(way, True).wait_recv()
        grad_passed(way, False).start()
    for way in (0, 1):
        grad_passed(way, True).wait_recv()

    lines = r["proj_out"].shape[0]
    per_part = nz // nx

    def term(t, carry):
        value = dot(r["out_grad"][:, columns(t)], r["mixed"][...], 0, 0)
        r["term"][pl.ds(t * per_part, per_part)] = value.reshape(
            per_part, ny, nc, lines, width
        ).astype(BF16)
        return carry

    lax.fori_loop(0, nx, term, 0)
    cut = lines // PIECES

    def rows_in(p):
        return pl.ds(p * cut, cut)

    def core_sum(p):
        return remote(
            r["term"].at[:, :, twin, rows_in(p), :],
            r["core_in"].at[:, :, rows_in(p), :],
            r["core_send"].at[p],
            r["core_recv"].at[p],
            (z, y, twin, x),
        )

    for p in range(PIECES):
        core_sum(p).start()

    r["d_mixed"][...] = jnp.zeros_like(r["d_mixed"])

    def mix(t, carry):
        cols = columns(t)
        r["d_mixed"][...] += dot(r["out_grad"][:, cols], r["out_proj_in"][cols, :])
        return carry

    lax.fori_loop(0, nx, mix, 0)
    d_mixed = r["d_mixed"][...]
    r["gate_grad"][...] = (d_mixed * r["by_gate"][...]).astype(BF16)
    local_grad = d_mixed * r["gate"][...]
    step, level = 1, 0
    while step < tokens:
        local_grad = local_grad + r["reach"][level] * pltpu.roll(local_grad, tokens - step, 0)
        step *= 2
        level += 1
    r["local_grad"][...] = local_grad
    head = r["first_decay"][0:1, :]
    link = jnp.concatenate(
        [
            head * r["carry_weight"][0:1, :],
            head * local_grad[0:1, :],
            jnp.zeros((6, width), F32),
        ],
        axis=0,
    )
    r["near_links"][mine] = link

    def near_link(j, arrives):
        _, py, pc = partner(j, -1 if arrives else 1)
        slot = py * nc + pc if arrives else mine
        here = r["near_links"].at[slot]
        return remote(here, here, r["near_send"].at[j], r["near_recv"].at[j], (z, py, pc, x))

    for j in range(1, plane):
        near_link(j, False).start()

    def up_half(p, way, arrives):
        half = nz // 2
        return remote(
            r["core_out"].at[pl.ds(way * half, half), over, rows_in(p), :],
            r["line_half"].at[way, :, rows_in(p), :],
            r["line_send"].at[way, p],
            r["line_recv"].at[way, p],
            (z, (down, up)[way] if arrives else (up, down)[way], c, x),
        )

    def up_unit(p, way, arrives):
        return remote(
            r["line_out"].at[way, :, rows_in(p), :],
            r["line_in"].at[way, :, rows_in(p), :],
            r["line_send"].at[2 + way, p],
            r["line_recv"].at[2 + way, p],
            (z, (down, up)[way] if arrives else (up, down)[way], c, x),
        )

    for p in range(PIECES):
        core_sum(p).wait_recv()

        def add(k, carry):
            value = r["term"][k, :, pl.ds(c, 1), rows_in(p), :].reshape(ny, cut, width)
            value = value.astype(F32) + r["core_in"][k, :, rows_in(p), :].astype(F32)
            r["core_out"][k, :, rows_in(p), :] = value.astype(BF16)
            return carry

        lax.fori_loop(0, nz, add, 0)
        for way in (0, 1):
            up_half(p, way, False).start()

    for j in range(1, plane):
        near_link(j, True).wait_recv()
    one, zero = jnp.ones((1, width), F32), jnp.zeros((1, width), F32)
    all_weight, all_start, near_weight, near_start = one, zero, one, zero
    for q in range(plane - 1, -1, -1):
        a, b = r["near_links"][q, 0:1, :], r["near_links"][q, 1:2, :]
        all_weight, all_start = a * all_weight, b + a * all_start
        later = q > mine
        near_start = jnp.where(later, b + a * near_start, near_start)
        near_weight = jnp.where(later, a * near_weight, near_weight)
    r["far_links"][z] = jnp.concatenate(
        [all_weight, all_start, jnp.zeros((6, width), F32)], axis=0
    )

    def far_link(dz, arrives):
        pz, _, _ = partner(dz * plane, -1 if arrives else 1)
        here = r["far_links"].at[pz if arrives else z]
        return remote(here, here, r["far_send"].at[dz], r["far_recv"].at[dz], (pz, y, c, x))

    for dz in range(1, nz):
        far_link(dz, False).start()

    for p in range(PIECES):
        for way in (0, 1):
            up_half(p, way, True).wait_recv()
            half = nz // 2
            target = (up, down)[way]
            for part in (0, 1):
                place = pl.ds(part * half, half)
                value = r["core_out"][place, target, rows_in(p), :].astype(F32)
                if part == way:
                    value = value + r["line_half"][way, :, rows_in(p), :].astype(F32)
                r["line_out"][way, place, rows_in(p), :] = value.astype(BF16)
            up_unit(p, way, False).start()

    def far_sum(p, dz, arrives):
        pz, _, _ = partner(dz * plane, -1 if arrives else 1)
        return remote(
            r["last_out"].at[z if arrives else pz, rows_in(p), :],
            r["last_in"].at[pz if arrives else z, rows_in(p), :],
            r["last_send"].at[p, dz],
            r["last_recv"].at[p, dz],
            (pz, y, c, x),
        )

    for p in range(PIECES):
        for way in (0, 1):
            up_unit(p, way, True).wait_recv()
        value = r["core_out"][:, y, rows_in(p), :].astype(F32)
        for way in (0, 1):
            value = value + r["line_in"][way, :, rows_in(p), :].astype(F32)
        r["last_out"][:, rows_in(p), :] = value.astype(BF16)
        for dz in range(1, nz):
            far_sum(p, dz, False).start()
        r["last_in"][z, rows_in(p), :] = r["last_out"][z, rows_in(p), :]

    for dz in range(1, nz):
        far_link(dz, True).wait_recv()
    far_start = zero
    for q in range(nz - 1, -1, -1):
        a, b = r["far_links"][q, 0:1, :], r["far_links"][q, 1:2, :]
        far_start = jnp.where(q > z, b + a * far_start, far_start)
    incoming = near_start + near_weight * far_start
    state_grad = r["local_grad"][...] + r["carry_weight"][...] * incoming
    d_recur = (state_grad * r["by_recur"][...]).astype(BF16)
    d_input = (state_grad * r["by_input"][...]).astype(BF16)
    through = dot(d_recur, r["recur_map_in"][0], 1, 1) + dot(d_input, r["input_map_in"][0], 1, 1)
    r["conv_grad"][...] = (state_grad * r["by_conv"][...] + through).astype(BF16)

    for p in range(PIECES):
        for dz in range(1, nz):
            far_sum(p, dz, True).wait_recv()
        r["proj_out"][rows_in(p), :] = jnp.sum(
            r["last_in"][:, rows_in(p), :].astype(F32), axis=0
        )

    def drain(j, carry):
        for k in (0, 1):
            sent(k, j).wait_send()
        returned(j).wait_send()
        return carry

    lax.fori_loop(1, experts, drain, 0)
    for dz in range(nz):
        for k, way in both_ways:
            own(k, dz, way, False).wait_send()
            passed(k, dz, way, False).wait_send()
        for way in (0, 1):
            half_sum(dz, way, False).wait_send()
            unit_sum(dz, way, False).wait_send()
    for way in (0, 1):
        grad_own(way, False).wait_send()
        grad_passed(way, False).wait_send()
    for j in range(1, plane):
        near_link(j, False).wait_send()
    for dz in range(1, nz):
        far_link(dz, False).wait_send()
    for p in range(PIECES):
        core_sum(p).wait_send()
        for way in (0, 1):
            up_half(p, way, False).wait_send()
            up_unit(p, way, False).wait_send()
        for dz in range(1, nz):
            far_sum(p, dz, False).wait_send()
    for name in ("gate", "up", "down"):
        stores[name].wait()


HELD = ("ids", "weights", "mixer", "cot")
RECURRENCE = (
    "recur_gate", "decay_rate", "norm", "conv", "input_gate", "states", "gate_pre",
)
LOADED = (*RECURRENCE, "w_gate", "w_up", "w_down", "out_proj", "recur_map", "input_map")
IN_NAMES = HELD + LOADED
OUT_NAMES = ("grad_gate", "grad_up", "grad_down", "proj_out", "conv_grad", "gate_grad")


def scratch_of(sizes, tokens, width, hidden, held):
    nz, ny, nc, nx = sizes
    plane = ny * nc
    experts = nz * plane
    capacity = 4 * tokens // experts
    features = nx * width
    lines = features // experts
    group = plane * capacity
    levels = tokens.bit_length() - 1
    dma = pltpu.SemaphoreType.DMA
    per_token = lambda kind: pltpu.VMEM((tokens, width), kind)
    shapes = {name + "_in": pltpu.VMEM(a.shape, a.dtype) for name, a in held.items()}
    shapes |= {
        "rows": pltpu.VMEM((experts, capacity, features), BF16),
        "cots": pltpu.VMEM((experts, capacity, features), BF16),
        "hits": pltpu.VMEM((experts * capacity, tokens), BF16),
        "send_rows": pltpu.VMEM((experts, capacity, width), BF16),
        "send_cots": pltpu.VMEM((experts, capacity, width), BF16),
        "acc_gate": pltpu.VMEM((2 * group, hidden), F32),
        "acc_up": pltpu.VMEM((2 * group, hidden), F32),
        "acc_down": pltpu.VMEM((2 * group, hidden), F32),
        "active": pltpu.VMEM((experts, capacity, hidden), BF16),
        "d_gate": pltpu.VMEM((experts, capacity, hidden), BF16),
        "d_up": pltpu.VMEM((experts, capacity, hidden), BF16),
        "partial": pltpu.VMEM((experts, capacity, features), BF16),
        "g_gate": pltpu.VMEM((features, hidden), BF16),
        "g_up": pltpu.VMEM((features, hidden), BF16),
        "g_down": pltpu.VMEM((hidden, features), BF16),
        "half_in": pltpu.VMEM((2, nz, plane // 2, capacity, width), BF16),
        "unit_out": pltpu.VMEM((2, nz, plane, capacity, width), BF16),
        "unit_in": pltpu.VMEM((2, nz, plane, capacity, width), BF16),
        "back_out": pltpu.VMEM((experts, capacity, width), BF16),
        "back_in": pltpu.VMEM((experts, capacity, width), BF16),
        "out_grad": pltpu.VMEM((tokens, features), BF16),
        "by_recur": per_token(F32),
        "by_input": per_token(F32),
        "by_conv": per_token(F32),
        "by_gate": per_token(F32),
        "gate": per_token(F32),
        "mixed": per_token(BF16),
        "first_decay": pltpu.VMEM((8, width), F32),
        "reach": pltpu.VMEM((levels, tokens, width), F32),
        "carry_weight": per_token(F32),
        "d_mixed": per_token(F32),
        "local_grad": per_token(F32),
        "term": pltpu.VMEM((nz, ny, nc, lines, width), BF16),
        "core_in": pltpu.VMEM((nz, ny, lines, width), BF16),
        "core_out": pltpu.VMEM((nz, ny, lines, width), BF16),
        "line_half": pltpu.VMEM((2, nz // 2, lines, width), BF16),
        "line_out": pltpu.VMEM((2, nz, lines, width), BF16),
        "line_in": pltpu.VMEM((2, nz, lines, width), BF16),
        "last_out": pltpu.VMEM((nz, lines, width), BF16),
        "last_in": pltpu.VMEM((nz, lines, width), BF16),
        "near_links": pltpu.VMEM((plane, 8, width), F32),
        "far_links": pltpu.VMEM((nz, 8, width), F32),
        "met": pltpu.SemaphoreType.REGULAR,
        "load_sem": dma((len(held),)),
        "store_sem": dma((3,)),
    }
    for name, shape in {
        "a": (2, experts),
        "own": (2, 2, nz),
        "pass": (2, 2, nz),
        "half": (2, nz),
        "unit": (2, nz),
        "back": (experts,),
        "og": (4,),
        "near": (plane,),
        "far": (nz,),
        "core": (PIECES,),
        "line": (4, PIECES),
        "last": (PIECES, nz),
    }.items():
        shapes[name + "_send"] = dma(shape)
        shapes[name + "_recv"] = dma(shape)
    return shapes


SIZES = (8, 4, 2, 4)
SCRATCH_NAMES = tuple(
    scratch_of(SIZES, 128, 512, 256, {n: jax.ShapeDtypeStruct((8, 128), F32) for n in LOADED})
)


def layer(held, loaded):
    sizes = tuple(lax.axis_size(a) for a in AXES)
    nz, ny, nc, nx = sizes
    tokens, width = held[3].shape
    named = dict(zip(LOADED, loaded, strict=True))
    hidden = named["w_gate"].shape[1]
    features = nx * width
    shapes = scratch_of(sizes, tokens, width, hidden, named)
    vmem = pl.BlockSpec(memory_space=pltpu.VMEM)
    left = pl.BlockSpec(memory_space=pl.ANY)
    return pl.pallas_call(
        functools.partial(layer_kernel, sizes),
        out_shape=(
            jax.ShapeDtypeStruct((features, hidden), BF16),
            jax.ShapeDtypeStruct((features, hidden), BF16),
            jax.ShapeDtypeStruct((hidden, features), BF16),
            jax.ShapeDtypeStruct((features // (nz * ny * nc), width), F32),
            jax.ShapeDtypeStruct((tokens, width), BF16),
            jax.ShapeDtypeStruct((tokens, width), BF16),
        ),
        in_specs=[vmem] * len(HELD) + [left] * len(LOADED),
        out_specs=(left,) * 3 + (vmem,) * 3,
        scratch_shapes=list(shapes.values()),
        compiler_params=pltpu.CompilerParams(
            collective_id=0, has_side_effects=True, vmem_limit_bytes=60 * 2**20
        ),
        name="layer",
    )(*held, *loaded)


def body(
    cotangent,
    mixer_out,
    route_ids,
    route_weights,
    conv_out,
    recur_gate,
    input_gate,
    gate_pre,
    states_before,
    decay_rate,
    out_proj,
    recur_map,
    input_map,
    expert_gate,
    expert_up,
    expert_down,
):
    row_count = cotangent.shape[0]
    rate = decay_rate[None, :]
    log_decay = -8.0 * recur_gate.astype(F32) * rate
    position = lax.axis_index(SP) * row_count + jnp.arange(row_count, dtype=jnp.int32)
    at_start = (position == 0)[:, None]
    norm_factor = jnp.where(at_start, 1.0, jnp.sqrt(-jnp.expm1(2.0 * log_decay)))
    grads = layer(
        (route_ids.T, route_weights.T, mixer_out, cotangent),
        (
            recur_gate,
            rate,
            norm_factor,
            conv_out,
            input_gate,
            states_before,
            gate_pre,
            expert_gate[0],
            expert_up[0],
            expert_down[0],
            out_proj,
            recur_map,
            input_map,
        ),
    )
    return (grads[0][None], grads[1][None], grads[2][None], *grads[3:])


def solution(mesh):
    torus = Mesh(mesh.devices.reshape(8, 4, 2, mesh.shape["tp"]), ("sp_0", "sp_1", "sp_2", "tp"))
    in_specs = (
        P(SP, "tp"),
        P(SP, "tp"),
        P(SP, None),
        P(SP, None),
        P(SP, "tp"),
        P(SP, "tp"),
        P(SP, "tp"),
        P(SP, "tp"),
        P(SP, "tp"),
        P("tp"),
        P(None, "tp"),
        P("tp", None, None),
        P("tp", None, None),
        P(SP, None, "tp"),
        P(SP, None, "tp"),
        P(SP, "tp", None),
    )
    out_specs = (
        P(SP, None, "tp"),
        P(SP, None, "tp"),
        P(SP, "tp", None),
        P(SP, "tp"),
        P(SP, "tp"),
        P(SP, "tp"),
    )
    return jax.shard_map(body, mesh=torus, in_specs=in_specs, out_specs=out_specs, check_vma=False)
```

time: 260 us -> 133 us (0.51)
  Pallas kernels: 0 us -> 123 us
  blocking collectives: 119 us -> 0 us
  starting transfers between devices: 33 us -> 0 us
  local copies, waits for them, and re-layouts: 39.2 us -> 6.31 us
  waiting for transfers between devices: 25.2 us -> 0 us
  matrix products: 22.1 us -> 0 us
  other arithmetic: 17.2 us -> 2.48 us
    pallas_call x0 -> x1, Pallas kernels: none -> 123 us  [layer(): pl.pallas_call(functools.partial(layer_kernel, sizes), out_shape=(jax.Sha...]
    all_to_all x3 -> x0, blocking collectives: 119 us -> none  [the longest x1 51 us: from_everyone(): lax.all_to_all(jnp.broadcast_to(shard[None], (devices, *shard.shape)), ax...]
    all_to_all x5 -> x0, starting transfers between devices: 33 us -> none  [the longest x1 9.87 us: body(): lax.all_to_all(summed, SP, split_axis=0, concat_axis=0, tiled=True)]
    all_to_all x5 -> x0, waiting for transfers between devices: 25.2 us -> none  [the longest x1 17.6 us: body(): lax.all_to_all(summed, SP, split_axis=0, concat_axis=0, tiled=True)]
    slice x76 -> x0, local copies, waits for them, and re-layouts: 22.1 us -> none  [the longest x24 18.6 us: joined_by_halves(): part[side::2]]
    dot_general x15 -> x0, matrix products: 22.1 us -> none  [the longest x5 11.2 us: contract_rows(): lax.dot_general(left, right, (((0,), (0,)), ((), ())), preferred_element_...]
    reduce_sum x5 -> x0, other arithmetic: 7.28 us -> none  [the longest x2 6.24 us: sent_and_summed(): return arrived.astype(jnp.float32).sum(axis=0)]
    mul x18 -> x1, other arithmetic: 6.18 us -> 0.69 us  [body(): log_decay = -8.0 * recur_gate.astype(F32) * rate]
  transfers between devices with their start and end apart: 5 -> 0, of which waited for: 4 -> 0; matrix products, arithmetic and copies ran while one was open for 18% -> 0% of each run, Pallas kernels for 0% -> 0%
where the time goes in v2:
time: 133 us; the launch traced here: 132 us
  Pallas kernels  123 us (92%)
  local copies, waits for them, and re-layouts  6.31 us (5%)
  other arithmetic  2.48 us (2%)
    pallas_call x1, Pallas kernels, layer(): pl.pallas_call(functools.partial(layer_kernel, sizes), out_shape=(jax.Sha...  123 us
    unnamed x16, local copies, waits for them, and re-layouts  6.31 us

profile of v2, /device:TPU:1, one launch (start us, length us, event | category | flops | bytes accessed | tf_op | source)
XLA Modules:
  0.0 132.4 jit_solution(13119165048214517424)
XLA Ops:
  0.7 0.7 broadcast_multiply_fusion
  1.3 1.8 %sqrt_select_fusion.refs_6_ = f32[128,512]{1,0:T(8,128)} fusion(bf16[128,512]{1,0:T(8,128)(2,1)} %refs_4_.1, f32[512]{0:T(512)S(1)} %broadcast_multiply_fusion, pred[128]{0:T(512)(128)(4,1)S(1)} %add_compare_fusion), kind=kLoop, calls=%fused_computation | loop fusion | flops 327680 | bytes 395392 | tf_op jit(solution)/shard_map/jit(_where)/select_n | solution.py:841
  3.1 123.0 %layer.1 = (bf16[2048,256]{1,0:T(8,128)(2,1)}, bf16[2048,256]{1,0:T(8,128)(2,1)}, bf16[256,2048]{1,0:T(8,128)(2,1)}, f32[32,512]{1,0:T(8,128)}, bf16[128,512]{1,0:T(8,128)(2,1)}, /*index=5*/bf16[128,512]{1,0:T(8,128)(2,1)}) custom-call(s32[2,128]{1,0:T(2,128)} %bitcast.16, f32[2,128]{1,0:T(2,128)} %bitcast.17, bf16[128,512]{1,0:T(8,128)(2,1)} %refs_2_.1, ...), custom_call_target="tpu_custom_call" | custom-call | tf_op jit(solution)/shard_map/layer/pallas_call | solution.py:798
  126.1 0.0 copy-start.1
  126.1 0.0 copy-start
  126.1 2.4 %copy.28 = bf16[1,2048,256]{2,1,0:T(8,128)(2,1)} copy(bf16[1,2048,256]{2,1,0:T(8,128)(2,1)} %bitcast.14) | data formatting | bytes 2097152
  128.5 0.0 copy-done.1
  128.5 0.0 copy-start.4
  128.5 0.0 copy-start.3
  128.5 0.0 copy-start.2
  128.5 1.0 copy.29
  129.5 0.0 copy-done
  129.5 1.0 copy.30
  130.5 0.0 copy-done.4
  130.5 0.6 copy.31
  131.1 0.0 copy-done.3
  131.1 0.7 copy.32
  131.8 0.0 copy-done.2
  131.8 0.7 copy.33
  (1 shorter events, 0.0 us)
Async XLA Ops:
  126.1 2.4 %copy-start.1 = (bf16[2048,256]{1,0:T(8,128)(2,1)S(1)}, bf16[2048,256]{1,0:T(8,128)(2,1)}, u32[]{:S(2)}) copy-start(bf16[2048,256]{1,0:T(8,128)(2,1)} %get-tuple-element.13) | copy-start | bytes 3145732
  126.1 3.4 %copy-start = (bf16[256,2048]{1,0:T(8,128)(2,1)S(1)}, bf16[256,2048]{1,0:T(8,128)(2,1)}, u32[]{:S(2)}) copy-start(bf16[256,2048]{1,0:T(8,128)(2,1)} %get-tuple-element.14) | copy-start | bytes 3145732
  128.5 2.0 %copy-start.4 = (f32[32,512]{1,0:T(8,128)S(1)}, f32[32,512]{1,0:T(8,128)}, u32[]{:S(2)}) copy-start(f32[32,512]{1,0:T(8,128)} %get-tuple-element.27) | copy-start | bytes 196612
  128.5 2.6 %copy-start.3 = (bf16[128,512]{1,0:T(8,128)(2,1)S(1)}, bf16[128,512]{1,0:T(8,128)(2,1)}, u32[]{:S(2)}) copy-start(bf16[128,512]{1,0:T(8,128)(2,1)} %get-tuple-element.28) | copy-start | bytes 393220
  128.5 3.2 %copy-start.2 = (bf16[128,512]{1,0:T(8,128)(2,1)S(1)}, bf16[128,512]{1,0:T(8,128)(2,1)}, u32[]{:S(2)}) copy-start(bf16[128,512]{1,0:T(8,128)(2,1)} %get-tuple-element.29) | copy-start | bytes 393220

commit v3 on v2

v3 whole, which is shorter than its diff:
```python
import functools
import types

import jax
import jax.numpy as jnp
from jax import lax
from jax.experimental import pallas as pl
from jax.experimental.pallas import tpu as pltpu
from jax.sharding import Mesh
from jax.sharding import PartitionSpec as P

SP = ("sp_0", "sp_1", "sp_2")
AXES = (*SP, "tp")
MESH_ID = pl.DeviceIdType.MESH
BF16 = jnp.bfloat16
F32 = jnp.float32


def near_first(count):
    return sorted(range(count), key=lambda k: (min(k, count - k), k))


def slot_hits(ids, experts, capacity):
    tokens = ids.shape[1]
    slots = experts * capacity
    first, second = ids[0:1, :], ids[1:2, :]
    expert = lax.broadcasted_iota(jnp.int32, (experts, tokens), 0)
    named = jnp.where((expert == first) | (expert == second), 1.0, 0.0).astype(jnp.bfloat16)
    at = lax.broadcasted_iota(jnp.int32, (tokens, tokens), 0)
    later = lax.broadcasted_iota(jnp.int32, (tokens, tokens), 1)
    earlier = jnp.where(at < later, 1.0, 0.0).astype(jnp.bfloat16)
    before = jnp.dot(named, earlier, preferred_element_type=jnp.float32)
    of_slot = lax.broadcasted_iota(jnp.int32, (slots, experts), 0)
    of_expert = lax.broadcasted_iota(jnp.int32, (slots, experts), 1)
    spread = jnp.where(of_slot // capacity == of_expert, 1.0, 0.0).astype(jnp.bfloat16)
    rank = jnp.dot(spread, before.astype(jnp.bfloat16), preferred_element_type=jnp.float32)
    slot = lax.broadcasted_iota(jnp.int32, (slots, tokens), 0)
    free = rank == (slot % capacity).astype(jnp.float32)
    return free & (slot // capacity == first), free & (slot // capacity == second)


def dot(left, right, at_left=1, at_right=0):
    return lax.dot_general(
        left, right, (((at_left,), (at_right,)), ((), ())), preferred_element_type=F32
    )


def expm1_of(v):
    series = jnp.ones_like(v)
    for n in range(11, 1, -1):
        series = 1.0 + v * series * (1.0 / n)
    return jnp.where(jnp.abs(v) < 0.5, v * series, jnp.exp(v) - 1.0)


def layer_kernel(sizes, *refs):
    names = IN_NAMES + OUT_NAMES + SCRATCH_NAMES
    r = types.SimpleNamespace(**dict(zip(names, refs, strict=True)))
    nz, ny, nc, nx = sizes
    plane = ny * nc
    experts = nz * plane
    z, y, c, x = (lax.axis_index(a) for a in AXES)
    tokens, width = r.cot_in.shape
    capacity = r.sending.shape[2]
    me = (z * ny + y) * nc + c
    mine = y * nc + c
    right, left = lax.rem(x + 1, nx), lax.rem(x + nx - 1, nx)
    across = lax.rem(x + 2, nx)
    up, down = lax.rem(y + 1, ny), lax.rem(y + ny - 1, ny)
    over = lax.rem(y + 2, ny)
    twin = nc - 1 - c
    group = plane * capacity
    order = near_first(nz)[1:] + [0]
    waits = []

    def columns(part):
        return pl.ds(pl.multiple_of(part * width, width), width)

    def partner(j, sign):
        dz, dy, dc = j // plane, (j // nc) % ny, j % nc
        return (
            lax.rem(z + sign * dz + nz, nz),
            lax.rem(y + sign * dy + ny, ny),
            lax.rem(c + sign * dc + nc, nc),
        )

    def remote(source, target, send, recv, device):
        return pltpu.make_async_remote_copy(
            src_ref=source,
            dst_ref=target,
            send_sem=send,
            recv_sem=recv,
            device_id=device,
            device_id_type=MESH_ID,
        )

    loads = {
        name: pltpu.make_async_copy(getattr(r, name), getattr(r, name + "_in"), r.load_sem.at[k])
        for k, name in enumerate(LOADED)
    }
    for name in LOADED:
        loads[name].start()

    barrier = pltpu.get_barrier_semaphore()

    def greet(sem, first, stop, step):
        def one(k, carry):
            pl.semaphore_signal(
                sem, inc=1, device_id=(*partner(k * step, 1), x), device_id_type=MESH_ID
            )
            return carry

        lax.fori_loop(first, stop, one, 0)

    greet(barrier, 1, nz, plane)
    greet(barrier, 1, plane, 1)
    for side in (left, right):
        pl.semaphore_signal(barrier, inc=1, device_id=(z, y, c, side), device_id_type=MESH_ID)

    for name in HELD:
        loads[name].wait()
    first, second = slot_hits(r.ids_in[...], experts, capacity)
    hits = jnp.where(first | second, 1.0, 0.0).astype(BF16)
    r.hits[...] = hits
    weights = r.weights_in[...]
    weight = jnp.sum(
        jnp.where(first, weights[0:1, :], 0.0) + jnp.where(second, weights[1:2, :], 0.0),
        axis=1,
        keepdims=True,
    )
    shape = (experts, capacity, width)
    r.sending[:, 0] = dot(hits, r.mixer_in[...]).reshape(shape).astype(BF16)
    r.sending[:, 1] = (dot(hits, r.cot_in[...]) * weight).reshape(shape).astype(BF16)

    pl.semaphore_wait(barrier, nz - 1 + plane - 1 + 2)
    greet(r.met, 1, plane, 1)
    pl.semaphore_wait(r.met, plane - 1)

    def only_wait(like, sem):
        return remote(like, like, sem, sem, (z, y, twin, x))

    def sent(j):
        dz, dy, dc = partner(j, 1)
        return remote(
            r.sending.at[(dz * ny + dy) * nc + dc],
            r.pack.at[me, :, :, columns(x)],
            r.a_send.at[0],
            r.a_recv.at[j // plane],
            (dz, dy, dc, x),
        )

    pltpu.make_async_copy(
        r.sending.at[me], r.pack.at[me, :, :, columns(x)], r.a_recv.at[0]
    ).start()
    for dz in order:

        def send(j, carry):
            sent(j).start()
            return carry

        lax.fori_loop(max(dz * plane, 1), (dz + 1) * plane, send, 0)

    for name in RECURRENCE:
        loads[name].wait()
    recur = r.recur_gate_in[...].astype(F32)
    rate = r.decay_rate_in[...]
    log_decay = -8.0 * recur * rate
    decay = jnp.exp(log_decay)
    position = lax.broadcasted_iota(jnp.int32, (tokens, width), 0)
    at_start = (position + me * tokens) == 0
    norm = jnp.where(at_start, 1.0, jnp.sqrt(-expm1_of(2.0 * log_decay)))
    slope = jnp.where(at_start, 0.0, -jnp.exp(2.0 * log_decay) / norm)
    conv = r.conv_in[...].astype(F32)
    entry = r.input_gate_in[...].astype(F32)
    drive = entry * conv
    before = r.states_in[...].astype(F32)
    state = decay * before + norm * drive
    r.by_recur[...] = (
        (decay * before + slope * drive) * (-8.0 * rate) * recur * (1.0 - recur)
    )
    r.by_input[...] = norm * conv * entry * (1.0 - entry)
    r.by_conv[...] = norm * entry
    pre = r.gate_pre_in[...].astype(F32)
    root = 0.7978845608028654
    bent = jnp.tanh(root * (pre + 0.044715 * (pre * pre * pre)))
    cdf = 0.5 * (1.0 + bent)
    gate = pre * cdf
    gelu_slope = cdf + 0.5 * pre * (1.0 - bent * bent) * root * (1.0 + 3.0 * 0.044715 * (pre * pre))
    r.gate[...] = gate
    r.mixed[...] = (state * gate).astype(BF16)
    r.by_gate[...] = state * gelu_slope
    r.first_decay[...] = decay[0:8, :]
    following = pltpu.roll(decay, tokens - 1, 0)
    last = position == tokens - 1
    reach = jnp.where(last, 0.0, following)
    carry_weight = jnp.where(last, 1.0, following)
    step = 1
    level = 0
    while step < tokens:
        r.reach[level] = reach
        moved = pltpu.roll(reach, tokens - step, 0)
        reach = reach * moved
        moved = pltpu.roll(carry_weight, tokens - step, 0)
        carry_weight = carry_weight * jnp.where(position < tokens - step, moved, 1.0)
        step *= 2
        level += 1
    r.carry_weight[...] = carry_weight
    for name in LOADED:
        if name not in HELD + RECURRENCE:
            loads[name].wait()

    def start_of(dz):
        return lax.rem(z - dz + nz, nz) * plane

    def ring_block(ref, dz, half, part):
        start, count = start_of(dz), plane
        if half is not None:
            count = plane // 2
            start = start + half * count
        return ref.at[pl.ds(start, count), ..., columns(part)]

    sides = (left, right)
    others = (right, left)

    def own(dz, way, arrives):
        here = ring_block(r.pack, dz, None, sides[way] if arrives else x)
        return remote(
            here, here, r.own_send.at[way, 0], r.own_recv.at[way, dz],
            (z, y, c, sides[way] if arrives else others[way]),
        )

    def passed(dz, way, arrives):
        here = ring_block(r.pack, dz, way, across if arrives else sides[way])
        return remote(
            here, here, r.hand_send.at[way, 0], r.hand_recv.at[way, dz],
            (z, y, c, sides[way] if arrives else others[way]),
        )

    def hand_on(dz):
        for way in (0, 1):
            own(dz, way, True).wait_recv()
            passed(dz, way, False).start()

    def settle(dz):
        for way in (0, 1):
            passed(dz, way, True).wait_recv()

    def as_rows(kind, starts, cols):
        return jnp.concatenate(
            [r.pack[pl.ds(s, plane), kind, :, cols].reshape(group, -1) for s in starts], axis=0
        )

    def keep(ref, starts, cols, value):
        for k, s in enumerate(starts):
            part = value[k * group : (k + 1) * group]
            ref[pl.ds(s, plane), :, cols] = part.reshape(plane, capacity, -1).astype(BF16)

    def expert_rows(dzs):
        starts = [start_of(dz) for dz in dzs]
        size = pl.ds(0, len(dzs) * group)
        sums_of = [acc.at[size] for acc in (r.acc_gate, r.acc_up, r.acc_down)]
        for acc in sums_of:
            acc[...] = jnp.zeros(acc.shape, F32)

        def gather(t, carry):
            cols = columns(t)
            row_part = as_rows(0, starts, cols)
            sums_of[0][...] += dot(row_part, r.w_gate_in[cols, :])
            sums_of[1][...] += dot(row_part, r.w_up_in[cols, :])
            cot_part = as_rows(1, starts, cols)
            sums_of[2][...] += dot(cot_part, r.w_down_in[:, cols], 1, 1)
            return carry

        lax.fori_loop(0, nx, gather, 0)
        pre_gate, pre_up, d_active = (acc[...] for acc in sums_of)
        sig = jax.nn.sigmoid(pre_gate)
        silu = pre_gate * sig
        silu_slope = sig * (1.0 + pre_gate * (1.0 - sig))
        d_gate = d_active * pre_up * silu_slope
        d_up = d_active * silu
        whole = slice(None)
        keep(r.active, starts, whole, silu * pre_up)
        keep(r.d_gate, starts, whole, d_gate)
        keep(r.d_up, starts, whole, d_up)
        d_gate, d_up = d_gate.astype(BF16), d_up.astype(BF16)

        def spread(t, carry):
            cols = columns(t)
            value = dot(d_gate, r.w_gate_in[cols, :], 1, 1)
            value += dot(d_up, r.w_up_in[cols, :], 1, 1)
            keep(r.partial, starts, cols, value)
            return carry

        lax.fori_loop(0, nx, spread, 0)

    def half_sum(dz, way, arrives):
        return remote(
            ring_block(r.partial, dz, way, across),
            r.half_in.at[way, dz],
            r.half_send.at[way, 0],
            r.half_recv.at[way, dz],
            (z, y, c, sides[way] if arrives else others[way]),
        )

    def unit_sum(dz, way, arrives):
        return remote(
            r.unit_out.at[way, dz],
            r.unit_in.at[way, dz],
            r.unit_send.at[way, 0],
            r.unit_recv.at[way, dz],
            (z, y, c, sides[way] if arrives else others[way]),
        )

    def sum_one(dz):
        for way in (0, 1):
            half_sum(dz, way, False).start()

    def sum_two(dz):
        start = start_of(dz)
        for way in (0, 1):
            half_sum(dz, way, True).wait_recv()
            value = r.partial[pl.ds(start, plane), :, columns(others[way])].astype(F32)
            more = r.half_in[way, dz].astype(F32)
            half = plane // 2
            parts = [value[:half], value[half:]]
            parts[way] = parts[way] + more
            r.unit_out[way, dz] = jnp.concatenate(parts, axis=0).astype(BF16)
            unit_sum(dz, way, False).start()

    def returned(j):
        dz, dy, dc = partner(j, -1)
        return remote(
            r.back_out.at[(dz * ny + dy) * nc + dc],
            r.back_in.at[me],
            r.back_send.at[0],
            r.back_recv.at[0],
            (dz, dy, dc, x),
        )

    def back_local():
        return pltpu.make_async_copy(
            r.back_out.at[me], r.back_in.at[me], r.back_recv.at[0]
        )

    def sum_three(dz):
        start = start_of(dz)
        value = r.partial[pl.ds(start, plane), :, columns(x)].astype(F32)
        for way in (0, 1):
            unit_sum(dz, way, True).wait_recv()
            value = value + r.unit_in[way, dz].astype(F32)
        r.back_out[pl.ds(start, plane)] = value.astype(BF16)

        def give(j, carry):
            returned(j).start()
            return carry

        lax.fori_loop(max(dz * plane, 1), (dz + 1) * plane, give, 0)
        if dz == 0:
            back_local().start()

    chunks = [order[k : k + 2] for k in range(0, nz - 2, 2)] + [[dz] for dz in order[-2:]]

    def sums(stage, k):
        for dz in chunks[k] if k >= 0 else ():
            stage(dz)

    def rows_of(ref):
        return ref[...].reshape(experts * capacity, -1)

    def packed(kind, cols):
        return r.pack[:, kind, :, cols].reshape(experts * capacity, -1)

    def grad_in(slope_ref, grad_ref, begin, end):
        def part(t, carry):
            cols = columns(t)
            grad_ref[cols, :] = dot(packed(0, cols), rows_of(slope_ref), 0, 0).astype(BF16)
            return carry

        lax.fori_loop(begin, end, part, 0)

    def grad_down(begin, end):
        def part(t, carry):
            cols = columns(t)
            r.grad_down[:, cols] = dot(rows_of(r.active), packed(1, cols), 0, 0).astype(BF16)
            return carry

        lax.fori_loop(begin, end, part, 0)

    for at, dz in enumerate(order):
        only_wait(ring_block(r.pack, dz, None, x), r.a_recv.at[dz]).wait_recv()
        for way in (0, 1):
            own(dz, way, False).start()
        if at:
            hand_on(order[at - 1])
        if at >= 2:
            settle(order[at - 2])
        if at >= 3 and at % 2:
            k = (at - 3) // 2
            sums(sum_two, k - 1)
            sums(sum_three, k - 2)
            expert_rows(chunks[k])
            sums(sum_one, k)
    hand_on(order[-1])
    k = len(chunks) - 2
    sums(sum_two, k - 1)
    sums(sum_three, k - 2)
    settle(order[-2])
    expert_rows(chunks[k])
    sums(sum_one, k)
    sums(sum_three, k - 1)
    settle(order[-1])
    expert_rows(chunks[k + 1])
    sums(sum_one, k + 1)
    sums(sum_two, k)
    grad_in(r.d_gate, r.grad_gate, 0, 2)
    sums(sum_two, k + 1)
    sums(sum_three, k)
    grad_in(r.d_gate, r.grad_gate, 2, nx)
    sums(sum_three, k + 1)
    grad_in(r.d_up, r.grad_up, 0, nx)

    only_wait(r.back_in, r.back_recv.at[0]).wait_recv()
    routed = dot(r.hits[...], r.back_in[...].reshape(experts * capacity, width), 0, 0)
    r.out_grad[:, columns(x)] = (r.cot_in[...].astype(F32) + routed).astype(BF16)

    half_rows = tokens // 2

    def grad_own(way, arrives):
        here = r.out_grad.at[:, columns(sides[way] if arrives else x)]
        return remote(
            here, here, r.og_send.at[way], r.og_recv.at[way],
            (z, y, c, sides[way] if arrives else others[way]),
        )

    def grad_passed(way, arrives):
        here = r.out_grad.at[
            pl.ds(way * half_rows, half_rows), columns(across if arrives else sides[way])
        ]
        return remote(
            here, here, r.og_send.at[2 + way], r.og_recv.at[2 + way],
            (z, y, c, sides[way] if arrives else others[way]),
        )

    for way in (0, 1):
        grad_own(way, False).start()

    lines = r.proj_out.shape[0]
    pair = nz // nx

    def planes(t):
        return pl.ds(t * pair, pair)

    def core_sum(t):
        return remote(
            r.term.at[planes(t), :, twin],
            r.core_in.at[planes(t)],
            r.core_send.at[t],
            r.core_recv.at[t],
            (z, y, twin, x),
        )

    def line_half(t, way, arrives):
        return remote(
            r.core_out.at[t * pair + way, over],
            r.line_half.at[way, t],
            r.line_send.at[way, t],
            r.line_recv.at[way, t],
            (z, (down, up)[way] if arrives else (up, down)[way], c, x),
        )

    def line_unit(t, way, arrives):
        return remote(
            r.line_out.at[way, planes(t)],
            r.line_in.at[way, planes(t)],
            r.line_send.at[2 + way, t],
            r.line_recv.at[2 + way, t],
            (z, (down, up)[way] if arrives else (up, down)[way], c, x),
        )

    def start_term(t):
        value = dot(r.out_grad[:, columns(t)], r.mixed[...], 0, 0)
        r.term[planes(t)] = value.reshape(pair, ny, nc, lines, width).astype(BF16)
        core_sum(t).start()

    def add_core(t):
        core_sum(t).wait_recv()
        for k in range(pair):
            row = t * pair + k
            value = r.term[row, :, pl.ds(c, 1)].reshape(ny, lines, width).astype(F32)
            r.core_out[row] = (value + r.core_in[row].astype(F32)).astype(BF16)
        for way in (0, 1):
            line_half(t, way, False).start()

    def add_half(t):
        for way in (0, 1):
            line_half(t, way, True).wait_recv()
            target = (up, down)[way]
            for k in range(pair):
                row = t * pair + k
                value = r.core_out[row, target].astype(F32)
                if k == way:
                    value = value + r.line_half[way, t].astype(F32)
                r.line_out[way, row] = value.astype(BF16)
            line_unit(t, way, False).start()

    def add_line(t):
        for way in (0, 1):
            line_unit(t, way, True).wait_recv()
        for k in range(pair):
            row = t * pair + k
            value = r.core_out[row, y].astype(F32)
            for way in (0, 1):
                value = value + r.line_in[way, row].astype(F32)
            r.last_out[row] = value.astype(BF16)

            @pl.when(row != z)
            def _():
                remote(
                    r.last_out.at[row],
                    r.last_in.at[z],
                    r.last_send.at[0],
                    r.last_recv.at[0],
                    (row, y, c, x),
                ).start()

    start_term(x)
    grad_down(0, 2)
    add_core(x)
    for way in (0, 1):
        grad_own(way, True).wait_recv()
        grad_passed(way, False).start()
    start_term(left)
    start_term(right)
    add_half(x)
    add_core(left)
    add_core(right)
    for way in (0, 1):
        grad_passed(way, True).wait_recv()
    start_term(across)

    r.d_mixed[...] = jnp.zeros_like(r.d_mixed)

    def mix(t, carry):
        cols = columns(t)
        r.d_mixed[...] += dot(r.out_grad[:, cols], r.out_proj_in[cols, :])
        return carry

    lax.fori_loop(0, nx, mix, 0)
    d_mixed = r.d_mixed[...]
    r.gate_grad[...] = (d_mixed * r.by_gate[...]).astype(BF16)
    local_grad = d_mixed * r.gate[...]
    step, level = 1, 0
    while step < tokens:
        local_grad = local_grad + r.reach[level] * pltpu.roll(local_grad, tokens - step, 0)
        step *= 2
        level += 1
    r.local_grad[...] = local_grad
    head = r.first_decay[0:1, :]
    link = jnp.concatenate(
        [
            head * r.carry_weight[0:1, :],
            head * local_grad[0:1, :],
            jnp.zeros((6, width), F32),
        ],
        axis=0,
    )
    r.near_links[mine] = link

    def near_link(j):
        _, py, pc = partner(j, 1)
        here = r.near_links.at[mine]
        return remote(here, here, r.near_send.at[0], r.near_recv.at[0], (z, py, pc, x))

    for j in range(1, plane):
        near_link(j).start()
    add_core(across)
    add_half(left)
    add_half(right)
    add_line(x)

    only_wait(r.near_links.at[pl.ds(0, plane - 1)], r.near_recv.at[0]).wait_recv()
    one, zero = jnp.ones((1, width), F32), jnp.zeros((1, width), F32)
    all_weight, all_start, near_weight, near_start = one, zero, one, zero
    for q in range(plane - 1, -1, -1):
        a, b = r.near_links[q, 0:1, :], r.near_links[q, 1:2, :]
        all_weight, all_start = a * all_weight, b + a * all_start
        later = q > mine
        near_start = jnp.where(later, b + a * near_start, near_start)
        near_weight = jnp.where(later, a * near_weight, near_weight)
    r.far_links[z] = jnp.concatenate(
        [all_weight, all_start, jnp.zeros((6, width), F32)], axis=0
    )

    def far_link(dz):
        pz, _, _ = partner(dz * plane, 1)
        here = r.far_links.at[z]
        return remote(here, here, r.far_send.at[0], r.far_recv.at[0], (pz, y, c, x))

    for dz in range(1, nz):
        far_link(dz).start()
    add_half(across)
    add_line(left)
    add_line(right)
    grad_down(2, nx)
    add_line(across)

    only_wait(r.far_links.at[pl.ds(0, nz - 1)], r.far_recv.at[0]).wait_recv()
    far_start = zero
    for q in range(nz - 1, -1, -1):
        a, b = r.far_links[q, 0:1, :], r.far_links[q, 1:2, :]
        far_start = jnp.where(q > z, b + a * far_start, far_start)
    incoming = near_start + near_weight * far_start
    state_grad = r.local_grad[...] + r.carry_weight[...] * incoming
    d_recur = (state_grad * r.by_recur[...]).astype(BF16)
    d_input = (state_grad * r.by_input[...]).astype(BF16)
    through = dot(d_recur, r.recur_map_in[0], 1, 1) + dot(d_input, r.input_map_in[0], 1, 1)
    r.conv_grad[...] = (state_grad * r.by_conv[...] + through).astype(BF16)

    only_wait(r.last_in.at[pl.ds(0, nz - 1)], r.last_recv.at[0]).wait_recv()
    total = r.last_out[z].astype(F32)
    for dz in range(1, nz):
        total = total + r.last_in[lax.rem(z + dz, nz)].astype(F32)
    r.proj_out[...] = total

    ahead = pl.ds(0, experts // 2)
    only_wait(r.sending.at[pl.ds(0, experts - 1)], r.a_send.at[0]).wait_send()
    only_wait(r.back_out.at[pl.ds(0, experts - 1)], r.back_send.at[0]).wait_send()
    for way in (0, 1):
        only_wait(r.pack.at[..., columns(x)], r.own_send.at[way, 0]).wait_send()
        only_wait(r.pack.at[ahead, :, :, columns(x)], r.hand_send.at[way, 0]).wait_send()
        only_wait(r.partial.at[ahead, :, columns(x)], r.half_send.at[way, 0]).wait_send()
        only_wait(r.unit_out.at[way], r.unit_send.at[way, 0]).wait_send()
        grad_own(way, False).wait_send()
        grad_passed(way, False).wait_send()
    only_wait(r.near_links.at[pl.ds(0, plane - 1)], r.near_send.at[0]).wait_send()
    only_wait(r.far_links.at[pl.ds(0, nz - 1)], r.far_send.at[0]).wait_send()
    for t in range(nx):
        core_sum(t).wait_send()
        for way in (0, 1):
            line_half(t, way, False).wait_send()
            line_unit(t, way, False).wait_send()
    only_wait(r.last_out.at[pl.ds(0, nz - 1)], r.last_send.at[0]).wait_send()


HELD = ("ids", "weights", "mixer", "cot")
RECURRENCE = (
    "recur_gate", "decay_rate", "conv", "input_gate", "states", "gate_pre",
)
LOADED = (*HELD, *RECURRENCE, "w_gate", "w_up", "w_down", "out_proj", "recur_map", "input_map")
IN_NAMES = LOADED
OUT_NAMES = ("grad_gate", "grad_up", "grad_down", "proj_out", "conv_grad", "gate_grad")


def scratch_of(sizes, tokens, width, hidden, held):
    nz, ny, nc, nx = sizes
    plane = ny * nc
    experts = nz * plane
    capacity = 4 * tokens // experts
    features = nx * width
    lines = features // experts
    group = plane * capacity
    levels = tokens.bit_length() - 1
    dma = pltpu.SemaphoreType.DMA
    per_token = lambda kind: pltpu.VMEM((tokens, width), kind)
    shapes = {name + "_in": pltpu.VMEM(a.shape, a.dtype) for name, a in held.items()}
    shapes |= dict(
        pack=pltpu.VMEM((experts, 2, capacity, features), BF16),
        sending=pltpu.VMEM((experts, 2, capacity, width), BF16),
        hits=pltpu.VMEM((experts * capacity, tokens), BF16),
        acc_gate=pltpu.VMEM((2 * group, hidden), F32),
        acc_up=pltpu.VMEM((2 * group, hidden), F32),
        acc_down=pltpu.VMEM((2 * group, hidden), F32),
        active=pltpu.VMEM((experts, capacity, hidden), BF16),
        d_gate=pltpu.VMEM((experts, capacity, hidden), BF16),
        d_up=pltpu.VMEM((experts, capacity, hidden), BF16),
        partial=pltpu.VMEM((experts, capacity, features), BF16),
        half_in=pltpu.VMEM((2, nz, plane // 2, capacity, width), BF16),
        unit_out=pltpu.VMEM((2, nz, plane, capacity, width), BF16),
        unit_in=pltpu.VMEM((2, nz, plane, capacity, width), BF16),
        back_out=pltpu.VMEM((experts, capacity, width), BF16),
        back_in=pltpu.VMEM((experts, capacity, width), BF16),
        out_grad=pltpu.VMEM((tokens, features), BF16),
        by_recur=per_token(F32),
        by_input=per_token(F32),
        by_conv=per_token(F32),
        by_gate=per_token(F32),
        gate=per_token(F32),
        mixed=per_token(BF16),
        first_decay=pltpu.VMEM((8, width), F32),
        reach=pltpu.VMEM((levels, tokens, width), F32),
        carry_weight=per_token(F32),
        d_mixed=per_token(F32),
        local_grad=per_token(F32),
        term=pltpu.VMEM((nz, ny, nc, lines, width), BF16),
        core_in=pltpu.VMEM((nz, ny, lines, width), BF16),
        core_out=pltpu.VMEM((nz, ny, lines, width), BF16),
        line_half=pltpu.VMEM((2, nx, lines, width), BF16),
        line_out=pltpu.VMEM((2, nz, lines, width), BF16),
        line_in=pltpu.VMEM((2, nz, lines, width), BF16),
        last_out=pltpu.VMEM((nz, lines, width), BF16),
        last_in=pltpu.VMEM((nz, lines, width), BF16),
        near_links=pltpu.VMEM((plane, 8, width), F32),
        far_links=pltpu.VMEM((nz, 8, width), F32),
        met=pltpu.SemaphoreType.REGULAR,
        load_sem=dma((len(held),)),
    )
    for name, shape in dict(
        a=(nz,),
        own=(2, nz),
        hand=(2, nz),
        half=(2, nz),
        unit=(2, nz),
        back=(1,),
        og=(4,),
        near=(1,),
        far=(1,),
        core=(nx,),
        line=(4, nx),
        last=(1,),
    ).items():
        for end in ("_send", "_recv"):
            shapes[name + end] = dma(shape)
    return shapes


SIZES = (8, 4, 2, 4)
SCRATCH_NAMES = tuple(
    scratch_of(SIZES, 128, 512, 256, {n: jax.ShapeDtypeStruct((8, 128), F32) for n in LOADED})
)


def layer(*loaded):
    sizes = tuple(lax.axis_size(a) for a in AXES)
    nz, ny, nc, nx = sizes
    named = dict(zip(LOADED, loaded, strict=True))
    tokens, width = loaded[3].shape
    hidden = named["w_gate"].shape[1]
    features = nx * width
    shapes = scratch_of(sizes, tokens, width, hidden, named)
    vmem = pl.BlockSpec(memory_space=pltpu.VMEM)
    left = pl.BlockSpec(memory_space=pltpu.HBM)
    return pl.pallas_call(
        functools.partial(layer_kernel, sizes),
        out_shape=tuple(
            pltpu.VMEM(shape, kind)
            for shape, kind in (
                ((features, hidden), BF16),
                ((features, hidden), BF16),
                ((hidden, features), BF16),
                ((features // (nz * ny * nc), width), F32),
                ((tokens, width), BF16),
                ((tokens, width), BF16),
            )
        ),
        in_specs=[left] * len(LOADED),
        out_specs=(vmem,) * len(OUT_NAMES),
        scratch_shapes=list(shapes.values()),
        compiler_params=pltpu.CompilerParams(
            collective_id=0, has_side_effects=True, vmem_limit_bytes=48 * 2**20
        ),
        name="layer",
    )(*(pltpu.with_memory_space_constraint(a, pltpu.HBM) for a in loaded))


def store_kernel(*refs):
    count = len(refs) // 2
    copies = [
        pltpu.make_async_copy(refs[k], refs[count + k], refs[-1].at[k]) for k in range(count)
    ]
    for copy in copies:
        copy.start()
    for copy in copies:
        copy.wait()


def stored(arrays):
    count = len(arrays)
    return pl.pallas_call(
        store_kernel,
        out_shape=tuple(jax.ShapeDtypeStruct(a.shape, a.dtype) for a in arrays),
        in_specs=[pl.BlockSpec(memory_space=pltpu.VMEM)] * count,
        out_specs=(pl.BlockSpec(memory_space=pl.ANY),) * count,
        scratch_shapes=[pltpu.SemaphoreType.DMA((count,))],
        name="store",
    )(*(pltpu.with_memory_space_constraint(a, pltpu.VMEM) for a in arrays))


def body(
    cotangent,
    mixer_out,
    route_ids,
    route_weights,
    conv_out,
    recur_gate,
    input_gate,
    gate_pre,
    states_before,
    decay_rate,
    out_proj,
    recur_map,
    input_map,
    expert_gate,
    expert_up,
    expert_down,
):
    grads = layer(
        route_ids.T,
        route_weights.T,
        mixer_out,
        cotangent,
        recur_gate,
        decay_rate[None, :],
        conv_out,
        input_gate,
        states_before,
        gate_pre,
        expert_gate[0],
        expert_up[0],
        expert_down[0],
        out_proj,
        recur_map,
        input_map,
    )
    grads = stored(grads)
    return (grads[0][None], grads[1][None], grads[2][None], *grads[3:])


def solution(mesh):
    torus = Mesh(mesh.devices.reshape(8, 4, 2, mesh.shape["tp"]), ("sp_0", "sp_1", "sp_2", "tp"))
    in_specs = (
        P(SP, "tp"),
        P(SP, "tp"),
        P(SP, None),
        P(SP, None),
        P(SP, "tp"),
        P(SP, "tp"),
        P(SP, "tp"),
        P(SP, "tp"),
        P(SP, "tp"),
        P("tp"),
        P(None, "tp"),
        P("tp", None, None),
        P("tp", None, None),
        P(SP, None, "tp"),
        P(SP, None, "tp"),
        P(SP, "tp", None),
    )
    out_specs = (
        P(SP, None, "tp"),
        P(SP, None, "tp"),
        P(SP, "tp", None),
        P(SP, "tp"),
        P(SP, "tp"),
        P(SP, "tp"),
    )
    return jax.shard_map(body, mesh=torus, in_specs=in_specs, out_specs=out_specs, check_vma=False)
```

time: 133 us -> 113 us (0.85)
  Pallas kernels: 123 us -> 111 us
  local copies, waits for them, and re-layouts: 6.31 us -> 0 us
  other arithmetic: 2.48 us -> 0 us
    pallas_call x1 -> x2, Pallas kernels: 123 us -> 111 us  [the longest x1 109 us: layer(): pl.pallas_call(functools.partial(layer_kernel, sizes), out_shape=tuple((p...]
    unnamed x16 -> x0, local copies, waits for them, and re-layouts: 6.31 us -> none
    select_n x1 -> x0, other arithmetic: 1.79 us -> none  [body(): jnp.where(at_start, 1.0, jnp.sqrt(-jnp.expm1(2.0 * log_decay)))]
where the time goes in v3:
time: 113 us; the launch traced here: 112 us
  Pallas kernels  111 us (98%)
    pallas_call x1, Pallas kernels, layer(): pl.pallas_call(functools.partial(layer_kernel, sizes), out_shape=tuple((p...  109 us

profile of v3, /device:TPU:1, one launch (start us, length us, event | category | flops | bytes accessed | tf_op | source)
XLA Modules:
  0.0 111.7 jit_solution(4133584180563190781)
XLA Ops:
  0.6 109.2 %layer.1 = (bf16[2048,256]{1,0:T(8,128)(2,1)S(1)}, bf16[2048,256]{1,0:T(8,128)(2,1)S(1)}, bf16[256,2048]{1,0:T(8,128)(2,1)S(1)}, f32[32,512]{1,0:T(8,128)S(1)}, ...) custom-call(s32[2,128]{1,0:T(2,128)} %bitcast.13, f32[2,128]{1,0:T(2,128)} %bitcast.14, ...), custom_call_target="tpu_custom_call" | custom-call | tf_op jit(solution)/shard_map/layer/pallas_call | solution.py:741
  109.8 1.8 %store.1 = (bf16[2048,256]{1,0:T(8,128)(2,1)}, bf16[2048,256]{1,0:T(8,128)(2,1)}, bf16[256,2048]{1,0:T(8,128)(2,1)}, f32[32,512]{1,0:T(8,128)}, bf16[128,512]{1,0:T(8,128)(2,1)}, /*index=5*/bf16[128,512]{1,0:T(8,128)(2,1)}) custom-call(bf16[2048,256]{1,0:T(8,128)(2,1)S(1)} %get-tuple-element.18.refs_0_, bf16[2048,256]{1,0:T(8,128)(2,1)S(1)} %get-tuple-element.19.refs_1_, ...), custom_call_target="tpu_custom_call" | custom-call | tf_op jit(solution)/shard_map/store/pallas_call | solution.py:777

commit v4 on v3

--- a/solution.py
+++ b/solution.py
@@ -59,7 +59,7 @@
     plane = ny * nc
     experts = nz * plane
     z, y, c, x = (lax.axis_index(a) for a in AXES)
-    tokens, width = r.cot_in.shape
+    tokens, width = r.mixed.shape
     capacity = r.sending.shape[2]
     me = (z * ny + y) * nc + c
     mine = y * nc + c
@@ -69,7 +69,9 @@
     over = lax.rem(y + 2, ny)
     twin = nc - 1 - c
     group = plane * capacity
-    order = near_first(nz)[1:] + [0]
+    wide = [0, 1, nz - 1]
+    ring = [dz for dz in near_first(nz) if dz not in wide]
+    ring = ring[2:] + ring[:2]
     waits = []
 
     def columns(part):
@@ -93,8 +95,11 @@
             device_id_type=MESH_ID,
         )
 
+    raw_own = [r.raw.at[k, :, columns(x)] for k in (0, 1)]
+    places = [getattr(r, name + "_in", None) for name in LOADED]
+    places[2:4] = raw_own
     loads = {
-        name: pltpu.make_async_copy(getattr(r, name), getattr(r, name + "_in"), r.load_sem.at[k])
+        name: pltpu.make_async_copy(getattr(r, name), places[k], r.load_sem.at[k])
         for k, name in enumerate(LOADED)
     }
     for name in LOADED:
@@ -127,9 +132,10 @@
         axis=1,
         keepdims=True,
     )
+    r.slot_weight[...] = jnp.broadcast_to(weight, r.slot_weight.shape)
     shape = (experts, capacity, width)
-    r.sending[:, 0] = dot(hits, r.mixer_in[...]).reshape(shape).astype(BF16)
-    r.sending[:, 1] = (dot(hits, r.cot_in[...]) * weight).reshape(shape).astype(BF16)
+    r.sending[:, 0] = dot(hits, raw_own[0][...]).reshape(shape).astype(BF16)
+    r.sending[:, 1] = (dot(hits, raw_own[1][...]) * weight).reshape(shape).astype(BF16)
 
     pl.semaphore_wait(barrier, nz - 1 + plane - 1 + 2)
     greet(r.met, 1, plane, 1)
@@ -148,10 +154,32 @@
             (dz, dy, dc, x),
         )
 
+    sides = (left, right)
+    others = (right, left)
+    half_rows = tokens // 2
+
+    def raw_sent(way, arrives):
+        here = r.raw.at[:, :, columns(sides[way] if arrives else x)]
+        return remote(
+            here, here, r.raw_send.at[way], r.raw_recv.at[way],
+            (z, y, c, sides[way] if arrives else others[way]),
+        )
+
+    def raw_passed(way, arrives):
+        here = r.raw.at[
+            :, pl.ds(way * half_rows, half_rows), columns(across if arrives else sides[way])
+        ]
+        return remote(
+            here, here, r.raw_send.at[2 + way], r.raw_recv.at[2 + way],
+            (z, y, c, sides[way] if arrives else others[way]),
+        )
+
+    for way in (0, 1):
+        raw_sent(way, False).start()
     pltpu.make_async_copy(
         r.sending.at[me], r.pack.at[me, :, :, columns(x)], r.a_recv.at[0]
     ).start()
-    for dz in order:
+    for dz in (*ring, *wide):
 
         def send(j, carry):
             sent(j).start()
@@ -208,6 +236,35 @@
         if name not in HELD + RECURRENCE:
             loads[name].wait()
 
+    def send_wide(kind, part):
+        cols = columns(part)
+        for k, dz in enumerate(wide):
+            to = lax.rem(z + dz, nz)
+            slots = pl.ds(pl.multiple_of(to * group, group), group)
+            picked = r.hits[slots, :]
+            for side in (0, 1):
+                value = dot(picked, r.raw[side, :, cols])
+                if side:
+                    value = value * r.slot_weight[slots, 0:1]
+                r.wide[kind, k, :, side] = value.reshape(plane, capacity, width).astype(BF16)
+            if dz == 0:
+                pltpu.make_async_copy(
+                    r.wide.at[kind, k, mine], r.pack.at[me, :, :, cols], r.wide_recv.at[kind, k]
+                ).start()
+
+            def give(j, carry):
+                _, py, pc = partner(j, 1)
+                remote(
+                    r.wide.at[kind, k, py * nc + pc],
+                    r.pack.at[me, :, :, cols],
+                    r.wide_send.at[kind],
+                    r.wide_recv.at[kind, k],
+                    (to, py, pc, x),
+                ).start()
+                return carry
+
+            lax.fori_loop(0 if dz else 1, plane, give, 0)
+
     def start_of(dz):
         return lax.rem(z - dz + nz, nz) * plane
 
@@ -218,20 +275,17 @@
             start = start + half * count
         return ref.at[pl.ds(start, count), ..., columns(part)]
 
-    sides = (left, right)
-    others = (right, left)
-
     def own(dz, way, arrives):
         here = ring_block(r.pack, dz, None, sides[way] if arrives else x)
         return remote(
-            here, here, r.own_send.at[way, 0], r.own_recv.at[way, dz],
+            here, here, r.own_send.at[way], r.own_recv.at[way, dz],
             (z, y, c, sides[way] if arrives else others[way]),
         )
 
     def passed(dz, way, arrives):
         here = ring_block(r.pack, dz, way, across if arrives else sides[way])
         return remote(
-            here, here, r.hand_send.at[way, 0], r.hand_recv.at[way, dz],
+            here, here, r.hand_send.at[way], r.hand_recv.at[way, dz],
             (z, y, c, sides[way] if arrives else others[way]),
         )
 
@@ -270,7 +324,7 @@
             sums_of[2][...] += dot(cot_part, r.w_down_in[:, cols], 1, 1)
             return carry
 
-        lax.fori_loop(0, nx, gather, 0)
+        lax.fori_loop(0, nx, gather, 0, unroll=True)
         pre_gate, pre_up, d_active = (acc[...] for acc in sums_of)
         sig = jax.nn.sigmoid(pre_gate)
         silu = pre_gate * sig
@@ -290,13 +344,13 @@
             keep(r.partial, starts, cols, value)
             return carry
 
-        lax.fori_loop(0, nx, spread, 0)
+        lax.fori_loop(0, nx, spread, 0, unroll=True)
 
     def half_sum(dz, way, arrives):
         return remote(
             ring_block(r.partial, dz, way, across),
             r.half_in.at[way, dz],
-            r.half_send.at[way, 0],
+            r.half_send.at[way],
             r.half_recv.at[way, dz],
             (z, y, c, sides[way] if arrives else others[way]),
         )
@@ -305,7 +359,7 @@
         return remote(
             r.unit_out.at[way, dz],
             r.unit_in.at[way, dz],
-            r.unit_send.at[way, 0],
+            r.unit_send.at[way],
             r.unit_recv.at[way, dz],
             (z, y, c, sides[way] if arrives else others[way]),
         )
@@ -357,7 +411,7 @@
         if dz == 0:
             back_local().start()
 
-    chunks = [order[k : k + 2] for k in range(0, nz - 2, 2)] + [[dz] for dz in order[-2:]]
+    chunks = [wide[:1], ring[0:2], wide[1:], ring[2:4], ring[4:]]
 
     def sums(stage, k):
         for dz in chunks[k] if k >= 0 else ():
@@ -385,32 +439,58 @@
 
         lax.fori_loop(begin, end, part, 0)
 
-    for at, dz in enumerate(order):
+    def arrived(dz):
         only_wait(ring_block(r.pack, dz, None, x), r.a_recv.at[dz]).wait_recv()
-        for way in (0, 1):
-            own(dz, way, False).start()
-        if at:
-            hand_on(order[at - 1])
-        if at >= 2:
-            settle(order[at - 2])
-        if at >= 3 and at % 2:
-            k = (at - 3) // 2
-            sums(sum_two, k - 1)
-            sums(sum_three, k - 2)
-            expert_rows(chunks[k])
-            sums(sum_one, k)
-    hand_on(order[-1])
-    k = len(chunks) - 2
-    sums(sum_two, k - 1)
-    sums(sum_three, k - 2)
-    settle(order[-2])
-    expert_rows(chunks[k])
-    sums(sum_one, k)
-    sums(sum_three, k - 1)
-    settle(order[-1])
-    expert_rows(chunks[k + 1])
-    sums(sum_one, k + 1)
+        if dz in wide:
+            for kind, part in enumerate((left, right, across)):
+                only_wait(ring_block(r.pack, dz, None, part), r.wide_recv.at[kind, wide.index(dz)]).wait_recv()
+        else:
+            for way in (0, 1):
+                own(dz, way, False).start()
+
+    def work(k):
+        expert_rows(chunks[k])
+        sums(sum_one, k)
+
+    for way in (0, 1):
+        raw_sent(way, True).wait_recv()
+        raw_passed(way, False).start()
+    for way in (0, 1):
+        send_wide(way, sides[way])
+    arrived(ring[0])
+    for way in (0, 1):
+        raw_passed(way, True).wait_recv()
+    send_wide(2, across)
+    arrived(ring[1])
+    hand_on(ring[0])
+    arrived(wide[0])
+    work(0)
+    arrived(ring[2])
+    hand_on(ring[1])
+    settle(ring[0])
+    arrived(ring[3])
+    hand_on(ring[2])
+    settle(ring[1])
+    sums(sum_two, 0)
+    work(1)
+    arrived(ring[4])
+    hand_on(ring[3])
+    settle(ring[2])
+    sums(sum_two, 1)
+    sums(sum_three, 0)
+    hand_on(ring[4])
+    for dz in wide[1:]:
+        arrived(dz)
+    work(2)
+    settle(ring[3])
+    sums(sum_three, 1)
+    work(3)
+    sums(sum_two, 2)
+    settle(ring[4])
+    work(4)
+    k = 3
     sums(sum_two, k)
+    sums(sum_three, 2)
     grad_in(r.d_gate, r.grad_gate, 0, 2)
     sums(sum_two, k + 1)
     sums(sum_three, k)
@@ -420,9 +500,7 @@
 
     only_wait(r.back_in, r.back_recv.at[0]).wait_recv()
     routed = dot(r.hits[...], r.back_in[...].reshape(experts * capacity, width), 0, 0)
-    r.out_grad[:, columns(x)] = (r.cot_in[...].astype(F32) + routed).astype(BF16)
-
-    half_rows = tokens // 2
+    r.out_grad[:, columns(x)] = (raw_own[1][...].astype(F32) + routed).astype(BF16)
 
     def grad_own(way, arrives):
         here = r.out_grad.at[:, columns(sides[way] if arrives else x)]
@@ -576,6 +654,7 @@
     add_half(left)
     add_half(right)
     add_line(x)
+    add_half(across)
 
     only_wait(r.near_links.at[pl.ds(0, plane - 1)], r.near_recv.at[0]).wait_recv()
     one, zero = jnp.ones((1, width), F32), jnp.zeros((1, width), F32)
@@ -597,12 +676,33 @@
 
     for dz in range(1, nz):
         far_link(dz).start()
-    add_half(across)
     add_line(left)
     add_line(right)
     grad_down(2, nx)
     add_line(across)
 
+    ahead = pl.ds(0, experts // 2)
+    ringed = len(ring) * plane
+    only_wait(r.sending.at[pl.ds(0, experts - 1)], r.a_send.at[0]).wait_send()
+    only_wait(r.back_out.at[pl.ds(0, experts - 1)], r.back_send.at[0]).wait_send()
+    for way in (0, 1):
+        only_wait(r.pack.at[pl.ds(0, ringed), :, :, columns(x)], r.own_send.at[way]).wait_send()
+        only_wait(r.pack.at[pl.ds(0, ringed // 2), :, :, columns(x)], r.hand_send.at[way]).wait_send()
+        only_wait(r.partial.at[ahead, :, columns(x)], r.half_send.at[way]).wait_send()
+        only_wait(r.unit_out.at[way], r.unit_send.at[way]).wait_send()
+        raw_sent(way, False).wait_send()
+        raw_passed(way, False).wait_send()
+        grad_own(way, False).wait_send()
+        grad_passed(way, False).wait_send()
+    far = pl.ds(0, len(wide) * plane - 1)
+    for kind in range(3):
+        only_wait(r.pack.at[far, :, :, columns(x)], r.wide_send.at[kind]).wait_send()
+    only_wait(r.near_links.at[pl.ds(0, plane - 1)], r.near_send.at[0]).wait_send()
+    for t in range(nx):
+        core_sum(t).wait_send()
+        for way in (0, 1):
+            line_half(t, way, False).wait_send()
+            line_unit(t, way, False).wait_send()
     only_wait(r.far_links.at[pl.ds(0, nz - 1)], r.far_recv.at[0]).wait_recv()
     far_start = zero
     for q in range(nz - 1, -1, -1):
@@ -621,23 +721,7 @@
         total = total + r.last_in[lax.rem(z + dz, nz)].astype(F32)
     r.proj_out[...] = total
 
-    ahead = pl.ds(0, experts // 2)
-    only_wait(r.sending.at[pl.ds(0, experts - 1)], r.a_send.at[0]).wait_send()
-    only_wait(r.back_out.at[pl.ds(0, experts - 1)], r.back_send.at[0]).wait_send()
-    for way in (0, 1):
-        only_wait(r.pack.at[..., columns(x)], r.own_send.at[way, 0]).wait_send()
-        only_wait(r.pack.at[ahead, :, :, columns(x)], r.hand_send.at[way, 0]).wait_send()
-        only_wait(r.partial.at[ahead, :, columns(x)], r.half_send.at[way, 0]).wait_send()
-        only_wait(r.unit_out.at[way], r.unit_send.at[way, 0]).wait_send()
-        grad_own(way, False).wait_send()
-        grad_passed(way, False).wait_send()
-    only_wait(r.near_links.at[pl.ds(0, plane - 1)], r.near_send.at[0]).wait_send()
     only_wait(r.far_links.at[pl.ds(0, nz - 1)], r.far_send.at[0]).wait_send()
-    for t in range(nx):
-        core_sum(t).wait_send()
-        for way in (0, 1):
-            line_half(t, way, False).wait_send()
-            line_unit(t, way, False).wait_send()
     only_wait(r.last_out.at[pl.ds(0, nz - 1)], r.last_send.at[0]).wait_send()
 
 
@@ -661,9 +745,16 @@
     levels = tokens.bit_length() - 1
     dma = pltpu.SemaphoreType.DMA
     per_token = lambda kind: pltpu.VMEM((tokens, width), kind)
-    shapes = {name + "_in": pltpu.VMEM(a.shape, a.dtype) for name, a in held.items()}
+    shapes = {
+        name + "_in": pltpu.VMEM(a.shape, a.dtype)
+        for name, a in held.items()
+        if name not in HELD[2:]
+    }
     shapes |= dict(
         pack=pltpu.VMEM((experts, 2, capacity, features), BF16),
+        raw=pltpu.VMEM((2, tokens, features), BF16),
+        slot_weight=pltpu.VMEM((experts * capacity, 128), F32),
+        wide=pltpu.VMEM((3, 3, plane, 2, capacity, width), BF16),
         sending=pltpu.VMEM((experts, 2, capacity, width), BF16),
         hits=pltpu.VMEM((experts * capacity, tokens), BF16),
         acc_gate=pltpu.VMEM((2 * group, hidden), F32),
@@ -703,22 +794,24 @@
         met=pltpu.SemaphoreType.REGULAR,
         load_sem=dma((len(held),)),
     )
-    for name, shape in dict(
-        a=(nz,),
-        own=(2, nz),
-        hand=(2, nz),
-        half=(2, nz),
-        unit=(2, nz),
-        back=(1,),
-        og=(4,),
-        near=(1,),
-        far=(1,),
-        core=(nx,),
-        line=(4, nx),
-        last=(1,),
+    for name, (send, recv) in dict(
+        a=((1,), (nz,)),
+        own=((2,), (2, nz)),
+        hand=((2,), (2, nz)),
+        half=((2,), (2, nz)),
+        unit=((2,), (2, nz)),
+        back=((1,), (1,)),
+        raw=((4,), (4,)),
+        wide=((3,), (3, 3)),
+        og=((4,), (4,)),
+        near=((1,), (1,)),
+        far=((1,), (1,)),
+        core=((nx,), (nx,)),
+        line=((4, nx), (4, nx)),
+        last=((1,), (1,)),
     ).items():
-        for end in ("_send", "_recv"):
-            shapes[name + end] = dma(shape)
+        shapes[name + "_send"] = dma(send)
+        shapes[name + "_recv"] = dma(recv)
     return shapes
 
 

time: 113 us -> 104 us (0.920)
  the two profiles are of different devices: /device:TPU:1 before, /device:TPU:4 now
where the time goes in v4:
time: 104 us
  Pallas kernels  104 us (100%)
    pallas_call x1, Pallas kernels, layer(): pl.pallas_call(functools.partial(layer_kernel, sizes), out_shape=tuple((p...  102 us

profile of v4, /device:TPU:4, one launch (start us, length us, event | category | flops | bytes accessed | tf_op | source)
XLA Modules:
  0.0 104.3 jit_solution(17623500973711204913)
XLA Ops:
  0.6 101.9 %layer.1 = (bf16[2048,256]{1,0:T(8,128)(2,1)S(1)}, bf16[2048,256]{1,0:T(8,128)(2,1)S(1)}, bf16[256,2048]{1,0:T(8,128)(2,1)S(1)}, f32[32,512]{1,0:T(8,128)S(1)}, ...) custom-call(s32[2,128]{1,0:T(2,128)} %bitcast.13, f32[2,128]{1,0:T(2,128)} %bitcast.14, ...), custom_call_target="tpu_custom_call" | custom-call | tf_op jit(solution)/shard_map/layer/pallas_call | solution.py:834
  102.5 1.8 %store.1 = (bf16[2048,256]{1,0:T(8,128)(2,1)}, bf16[2048,256]{1,0:T(8,128)(2,1)}, bf16[256,2048]{1,0:T(8,128)(2,1)}, f32[32,512]{1,0:T(8,128)}, bf16[128,512]{1,0:T(8,128)(2,1)}, /*index=5*/bf16[128,512]{1,0:T(8,128)(2,1)}) custom-call(bf16[2048,256]{1,0:T(8,128)(2,1)S(1)} %get-tuple-element.18.refs_0_, bf16[2048,256]{1,0:T(8,128)(2,1)S(1)} %get-tuple-element.19.refs_1_, ...), custom_call_target="tpu_custom_call" | custom-call | tf_op jit(solution)/shard_map/store/pallas_call | solution.py:870

commit v5 on v4

--- a/solution.py
+++ b/solution.py
@@ -158,24 +158,25 @@
     others = (right, left)
     half_rows = tokens // 2
 
-    def raw_sent(way, arrives):
-        here = r.raw.at[:, :, columns(sides[way] if arrives else x)]
-        return remote(
-            here, here, r.raw_send.at[way], r.raw_recv.at[way],
-            (z, y, c, sides[way] if arrives else others[way]),
-        )
-
-    def raw_passed(way, arrives):
-        here = r.raw.at[
-            :, pl.ds(way * half_rows, half_rows), columns(across if arrives else sides[way])
-        ]
-        return remote(
-            here, here, r.raw_send.at[2 + way], r.raw_recv.at[2 + way],
-            (z, y, c, sides[way] if arrives else others[way]),
-        )
-
-    for way in (0, 1):
-        raw_sent(way, False).start()
+    def ring_gather(view, send, recv):
+        def step(kind, way, arrives):
+            half = 1 - way if kind == 1 else way
+            if kind == 2:
+                part = across if arrives else sides[way]
+            else:
+                part = sides[way] if arrives else x
+            here = view(pl.ds(half * half_rows, half_rows), columns(part))
+            return remote(
+                here, here, send.at[kind, way], recv.at[kind, way],
+                (z, y, c, sides[way] if arrives else others[way]),
+            )
+
+        return step
+
+    raw_step = ring_gather(lambda rows, cols: r.raw.at[:, rows, cols], r.raw_send, r.raw_recv)
+    for kind in (0, 1):
+        for way in (0, 1):
+            raw_step(kind, way, False).start()
     pltpu.make_async_copy(
         r.sending.at[me], r.pack.at[me, :, :, columns(x)], r.a_recv.at[0]
     ).start()
@@ -411,7 +412,7 @@
         if dz == 0:
             back_local().start()
 
-    chunks = [wide[:1], ring[0:2], wide[1:], ring[2:4], ring[4:]]
+    chunks = [wide[:1], ring[0:2], ring[2:3], wide[1:], ring[3:]]
 
     def sums(stage, k):
         for dz in chunks[k] if k >= 0 else ():
@@ -453,13 +454,14 @@
         sums(sum_one, k)
 
     for way in (0, 1):
-        raw_sent(way, True).wait_recv()
-        raw_passed(way, False).start()
+        raw_step(0, way, True).wait_recv()
+        raw_step(2, way, False).start()
     for way in (0, 1):
+        raw_step(1, way, True).wait_recv()
         send_wide(way, sides[way])
     arrived(ring[0])
     for way in (0, 1):
-        raw_passed(way, True).wait_recv()
+        raw_step(2, way, True).wait_recv()
     send_wide(2, across)
     arrived(ring[1])
     hand_on(ring[0])
@@ -471,55 +473,42 @@
     arrived(ring[3])
     hand_on(ring[2])
     settle(ring[1])
+    arrived(ring[4])
     sums(sum_two, 0)
-    work(1)
-    arrived(ring[4])
+    expert_rows(chunks[1])
     hand_on(ring[3])
+    sums(sum_one, 1)
     settle(ring[2])
+    hand_on(ring[4])
+    expert_rows(chunks[2])
     sums(sum_two, 1)
+    sums(sum_one, 2)
     sums(sum_three, 0)
-    hand_on(ring[4])
     for dz in wide[1:]:
         arrived(dz)
-    work(2)
+    work(3)
     settle(ring[3])
-    sums(sum_three, 1)
-    work(3)
-    sums(sum_two, 2)
     settle(ring[4])
     work(4)
-    k = 3
-    sums(sum_two, k)
+    sums(sum_three, 1)
+    sums(sum_two, 2)
+    sums(sum_two, 3)
+    grad_in(r.d_gate, r.grad_gate, 0, 2)
+    sums(sum_two, 4)
     sums(sum_three, 2)
-    grad_in(r.d_gate, r.grad_gate, 0, 2)
-    sums(sum_two, k + 1)
-    sums(sum_three, k)
+    sums(sum_three, 3)
     grad_in(r.d_gate, r.grad_gate, 2, nx)
-    sums(sum_three, k + 1)
+    sums(sum_three, 4)
     grad_in(r.d_up, r.grad_up, 0, nx)
 
     only_wait(r.back_in, r.back_recv.at[0]).wait_recv()
     routed = dot(r.hits[...], r.back_in[...].reshape(experts * capacity, width), 0, 0)
     r.out_grad[:, columns(x)] = (raw_own[1][...].astype(F32) + routed).astype(BF16)
 
-    def grad_own(way, arrives):
-        here = r.out_grad.at[:, columns(sides[way] if arrives else x)]
-        return remote(
-            here, here, r.og_send.at[way], r.og_recv.at[way],
-            (z, y, c, sides[way] if arrives else others[way]),
-        )
-
-    def grad_passed(way, arrives):
-        here = r.out_grad.at[
-            pl.ds(way * half_rows, half_rows), columns(across if arrives else sides[way])
-        ]
-        return remote(
-            here, here, r.og_send.at[2 + way], r.og_recv.at[2 + way],
-            (z, y, c, sides[way] if arrives else others[way]),
-        )
-
-    for way in (0, 1):
-        grad_own(way, False).start()
+    grad_step = ring_gather(lambda rows, cols: r.out_grad.at[rows, cols], r.og_send, r.og_recv)
+    for kind in (0, 1):
+        for way in (0, 1):
+            grad_step(kind, way, False).start()
 
     lines = r.proj_out.shape[0]
     pair = nz // nx
@@ -604,15 +593,16 @@
     grad_down(0, 2)
     add_core(x)
     for way in (0, 1):
-        grad_own(way, True).wait_recv()
-        grad_passed(way, False).start()
-    start_term(left)
-    start_term(right)
+        grad_step(0, way, True).wait_recv()
+        grad_step(2, way, False).start()
     add_half(x)
+    for way in (0, 1):
+        grad_step(1, way, True).wait_recv()
+        start_term(sides[way])
     add_core(left)
     add_core(right)
     for way in (0, 1):
-        grad_passed(way, True).wait_recv()
+        grad_step(2, way, True).wait_recv()
     start_term(across)
 
     r.d_mixed[...] = jnp.zeros_like(r.d_mixed)
@@ -653,7 +643,6 @@
     add_core(across)
     add_half(left)
     add_half(right)
-    add_line(x)
     add_half(across)
 
     only_wait(r.near_links.at[pl.ds(0, plane - 1)], r.near_recv.at[0]).wait_recv()
@@ -676,6 +665,7 @@
 
     for dz in range(1, nz):
         far_link(dz).start()
+    add_line(x)
     add_line(left)
     add_line(right)
     grad_down(2, nx)
@@ -690,10 +680,9 @@
         only_wait(r.pack.at[pl.ds(0, ringed // 2), :, :, columns(x)], r.hand_send.at[way]).wait_send()
         only_wait(r.partial.at[ahead, :, columns(x)], r.half_send.at[way]).wait_send()
         only_wait(r.unit_out.at[way], r.unit_send.at[way]).wait_send()
-        raw_sent(way, False).wait_send()
-        raw_passed(way, False).wait_send()
-        grad_own(way, False).wait_send()
-        grad_passed(way, False).wait_send()
+        for kind in range(3):
+            raw_step(kind, way, False).wait_send()
+            grad_step(kind, way, False).wait_send()
     far = pl.ds(0, len(wide) * plane - 1)
     for kind in range(3):
         only_wait(r.pack.at[far, :, :, columns(x)], r.wide_send.at[kind]).wait_send()
@@ -801,9 +790,9 @@
         half=((2,), (2, nz)),
         unit=((2,), (2, nz)),
         back=((1,), (1,)),
-        raw=((4,), (4,)),
+        raw=((3, 2), (3, 2)),
         wide=((3,), (3, 3)),
-        og=((4,), (4,)),
+        og=((3, 2), (3, 2)),
         near=((1,), (1,)),
         far=((1,), (1,)),
         core=((nx,), (nx,)),

time: 104 us -> 102 us (0.981)
  the two profiles are of different devices: /device:TPU:4 before, /device:TPU:1 now
where the time goes in v5:
time: 102 us
  Pallas kernels  101 us (99%)
    pallas_call x1, Pallas kernels, layer(): pl.pallas_call(functools.partial(layer_kernel, sizes), out_shape=tuple((p...  99.3 us

profile of v5, /device:TPU:1, one launch (start us, length us, event | category | flops | bytes accessed | tf_op | source)
XLA Modules:
  0.0 101.8 jit_solution(10003448298109201457)
XLA Ops:
  0.6 99.3 %layer.1 = (bf16[2048,256]{1,0:T(8,128)(2,1)S(1)}, bf16[2048,256]{1,0:T(8,128)(2,1)S(1)}, bf16[256,2048]{1,0:T(8,128)(2,1)S(1)}, f32[32,512]{1,0:T(8,128)S(1)}, ...) custom-call(s32[2,128]{1,0:T(2,128)} %bitcast.13, f32[2,128]{1,0:T(2,128)} %bitcast.14, ...), custom_call_target="tpu_custom_call" | custom-call | tf_op jit(solution)/shard_map/layer/pallas_call | solution.py:823
  99.9 1.8 %store.1 = (bf16[2048,256]{1,0:T(8,128)(2,1)}, bf16[2048,256]{1,0:T(8,128)(2,1)}, bf16[256,2048]{1,0:T(8,128)(2,1)}, f32[32,512]{1,0:T(8,128)}, bf16[128,512]{1,0:T(8,128)(2,1)}, /*index=5*/bf16[128,512]{1,0:T(8,128)(2,1)}) custom-call(bf16[2048,256]{1,0:T(8,128)(2,1)S(1)} %get-tuple-element.18.refs_0_, bf16[2048,256]{1,0:T(8,128)(2,1)S(1)} %get-tuple-element.19.refs_1_, ...), custom_call_target="tpu_custom_call" | custom-call | tf_op jit(solution)/shard_map/store/pallas_call | solution.py:859

commit v6 on v5

--- a/solution.py
+++ b/solution.py
@@ -589,9 +589,14 @@
                     (row, y, c, x),
                 ).start()
 
+    def mix(t):
+        cols = columns(t)
+        return dot(r.out_grad[:, cols], r.out_proj_in[cols, :])
+
     start_term(x)
     grad_down(0, 2)
     add_core(x)
+    r.d_mixed[...] = mix(x)
     for way in (0, 1):
         grad_step(0, way, True).wait_recv()
         grad_step(2, way, False).start()
@@ -599,21 +604,14 @@
     for way in (0, 1):
         grad_step(1, way, True).wait_recv()
         start_term(sides[way])
+    r.d_mixed[...] += mix(left) + mix(right)
     add_core(left)
     add_core(right)
     for way in (0, 1):
         grad_step(2, way, True).wait_recv()
     start_term(across)
 
-    r.d_mixed[...] = jnp.zeros_like(r.d_mixed)
-
-    def mix(t, carry):
-        cols = columns(t)
-        r.d_mixed[...] += dot(r.out_grad[:, cols], r.out_proj_in[cols, :])
-        return carry
-
-    lax.fori_loop(0, nx, mix, 0)
-    d_mixed = r.d_mixed[...]
+    d_mixed = r.d_mixed[...] + mix(across)
     r.gate_grad[...] = (d_mixed * r.by_gate[...]).astype(BF16)
     local_grad = d_mixed * r.gate[...]
     step, level = 1, 0

time: 102 us -> 102 us (level)
  no operation moved by 1% of the time
where the time goes in v6:
time: 102 us
  Pallas kernels  101 us (99%)
    pallas_call x1, Pallas kernels, layer(): pl.pallas_call(functools.partial(layer_kernel, sizes), out_shape=tuple((p...  99 us

profile of v6, /device:TPU:1, one launch (start us, length us, event | category | flops | bytes accessed | tf_op | source)
XLA Modules:
  0.0 101.6 jit_solution(1653226224478648648)
XLA Ops:
  0.6 99.0 %layer.1 = (bf16[2048,256]{1,0:T(8,128)(2,1)S(1)}, bf16[2048,256]{1,0:T(8,128)(2,1)S(1)}, bf16[256,2048]{1,0:T(8,128)(2,1)S(1)}, f32[32,512]{1,0:T(8,128)S(1)}, ...) custom-call(s32[2,128]{1,0:T(2,128)} %bitcast.13, f32[2,128]{1,0:T(2,128)} %bitcast.14, ...), custom_call_target="tpu_custom_call" | custom-call | tf_op jit(solution)/shard_map/layer/pallas_call | solution.py:821
  99.6 1.8 %store.1 = (bf16[2048,256]{1,0:T(8,128)(2,1)}, bf16[2048,256]{1,0:T(8,128)(2,1)}, bf16[256,2048]{1,0:T(8,128)(2,1)}, f32[32,512]{1,0:T(8,128)}, bf16[128,512]{1,0:T(8,128)(2,1)}, /*index=5*/bf16[128,512]{1,0:T(8,128)(2,1)}) custom-call(bf16[2048,256]{1,0:T(8,128)(2,1)S(1)} %get-tuple-element.18.refs_0_, bf16[2048,256]{1,0:T(8,128)(2,1)S(1)} %get-tuple-element.19.refs_1_, ...), custom_call_target="tpu_custom_call" | custom-call | tf_op jit(solution)/shard_map/store/pallas_call | solution.py:857
